TPU v7x, 32 devices: a whole 2x2x4 slice. The times are simulated.
32 devices in a mesh: fs: 4 (over z), rep: 4 (over y, x), tp: 2 (over core).
Axes of the slice: x: 2, y: 2, z: 4, core: 2. Of those that a mesh axis runs over, the one named last changes fastest.
Arguments:
- inputs: bfloat16 [4096, 2048], P(('fs', 'rep')), may hold values from -6 to 6
- cot_query: bfloat16 [4096, 2048], P(('fs', 'rep'), 'tp'), may hold values from -0.09375 to 0.09375
- cot_key: bfloat16 [4096, 512], P(('fs', 'rep'), 'tp'), may hold values from -0.09375 to 0.09375
- basis_query: bfloat16 [2048, 512], P('fs'), may hold values from -0.125 to 0.125
- basis_key: bfloat16 [2048, 512], P('fs'), may hold values from -0.125 to 0.125
- weight_query: float32 [2048, 2048], P('fs', 'tp'), may hold values from -0.125 to 0.125
- weight_key: float32 [2048, 512], P('fs', 'tp'), may hold values from -0.125 to 0.125
- moments_query: float32 [2, 512, 2048], P(None, 'fs', 'tp'), may hold values from -8 to 8, as said below
- moments_key: float32 [2, 512, 512], P(None, 'fs', 'tp'), may hold values from -8 to 8, as said below
Outputs:
- step_query: float32 [2048, 2048], P('fs', 'tp')
- step_key: float32 [2048, 512], P('fs', 'tp')
- new_weight_query: float32 [2048, 2048], P('fs', 'tp')
- new_weight_key: float32 [2048, 512], P('fs', 'tp')
- copy_query: bfloat16 [2048, 2048], P(None, 'tp')
- copy_key: bfloat16 [2048, 512], P(None, 'tp')
- new_moments_query: float32 [2, 512, 2048], P(None, 'fs', 'tp')
- new_moments_key: float32 [2, 512, 512], P(None, 'fs', 'tp')
Inputs may be any that keep to these rules, and one draw needn't show every extreme that they name: `moments_query`: entry 1 along the first dimension is positive. `moments_key`: entry 1 along the first dimension is positive.
All inputs are finite; a program needn't handle non-finite values.
Results may differ from a plain program's by a relative error of at most 0.009.
Values may be sent and summed in bfloat16 or wider, within the bound.
A program may use at most 64 MiB of HBM per device.

v0:
```python
import functools
import jax
import jax.numpy as jnp
from jax import lax
from jax.experimental import pallas as pl
from jax.experimental.pallas import tpu as pltpu
from jax.sharding import PartitionSpec as P

MESH = pl.DeviceIdType.MESH
LANES = 128


def each(start, stop, body):
    if stop - start <= 4:
        for i in range(start, stop):
            body(i)
    else:
        lax.fori_loop(start, stop, lambda i, carry: (body(i), carry)[1], 0)


def remote(src, dst, send_sem, recv_sem, **device):
    return pltpu.make_async_remote_copy(
        src_ref=src,
        dst_ref=dst,
        send_sem=send_sem,
        recv_sem=recv_sem,
        device_id=device,
        device_id_type=MESH,
    )


def exchange(
    fs,
    rep,
    inputs_far,
    cot_query_far,
    cot_key_far,
    basis_query,
    basis_key,
    full_query,
    full_key,
    moments_query_far,
    moments_key_far,
    basis_all,
    weight_query_all,
    weight_key_all,
    dir_query,
    dir_key,
    low_query,
    low_key,
    totals,
    inputs,
    cot_query,
    cot_key,
    moments_query,
    moments_key,
    loaded_query,
    loaded_key,
    wide_query,
    wide_key,
    factor,
    part_send,
    part_recv,
    slab,
    slab_recv,
    low_all,
    squares,
    pair,
    az_s,
    az_r,
    ap_s,
    ap_r,
    ez_s,
    ez_r,
    ep_s,
    ep_r,
    bp_s,
    bp_r,
    bz_s,
    bz_r,
    lp_s,
    lp_r,
    dr_s,
    dl_s,
    dz_r,
    qz_s,
    qz_r,
    pair_s,
    pair_r,
    local,
):
    f, r, c = lax.axis_index("fs"), lax.axis_index("rep"), lax.axis_index("tp")
    height = basis_query.shape[0]
    part = height // rep
    rank = basis_query.shape[1]
    rows = rank // fs
    tokens = inputs.shape[0]
    per = part_send.shape[0] // rep
    query_units = cot_query.shape[1] // LANES
    units = query_units + cot_key.shape[1] // LANES

    def ahead(i):
        return lax.rem(f + i, fs)

    def behind(i):
        return lax.rem(f + fs - i, fs)

    def beside(j):
        return lax.rem(r + j, rep)

    near = r + 1 - 2 * lax.rem(r, 2)
    far = r + 2 - 4 * (r // 2)
    across = 3 - r
    owners = (r, r, near, far)
    targets = (near, far, far, near)
    senders = (near, far, across, across)

    def span_of(slot, width):
        return (pl.ds(0, width), pl.ds(0, width), pl.ds(0, width // 2), pl.ds(width // 2, width // 2))[slot]

    def piece(source, owner):
        return pl.ds(pl.multiple_of(source * height + owner * part, part), part)

    own_part = pl.ds(pl.multiple_of(r * part, part), part)
    own_block = pl.ds(pl.multiple_of(f * height, height), height)

    def low_rows(source):
        return pl.ds(pl.multiple_of(source * rows, rows), rows)

    loads = [
        pltpu.make_async_copy(source, target, local.at[3 + n])
        for n, (source, target) in enumerate(
            (
                (full_query, loaded_query),
                (full_key, loaded_key),
                (inputs_far, inputs),
                (cot_query_far, cot_query),
                (cot_key_far, cot_key),
                (moments_query_far, moments_query),
                (moments_key_far, moments_key),
            )
        )
    ]
    barrier = pltpu.get_barrier_semaphore()

    def greet_fs(i):
        pl.semaphore_signal(barrier, inc=1, device_id={"fs": ahead(i)}, device_id_type=MESH)

    def greet_rep(j):
        pl.semaphore_signal(barrier, inc=1, device_id={"rep": beside(j)}, device_id_type=MESH)

    each(1, fs, greet_fs)
    each(1, rep, greet_rep)
    pl.semaphore_signal(barrier, inc=1, device_id={"tp": 1 - c}, device_id_type=MESH)
    pl.semaphore_wait(barrier, fs + rep - 1)

    bases = (basis_query, basis_key)
    weights = ((wide_query, weight_query_all), (wide_key, weight_key_all))

    def basis_fs(x, source, target):
        return remote(
            bases[x].at[own_part],
            basis_all.at[c, piece(source, r)],
            az_s.at[target],
            az_r.at[source],
            fs=target,
        )

    for x in range(2):

        @pl.when(c == x)
        def start_basis():
            each(1, fs, lambda i: basis_fs(x, f, ahead(i)).start())
            pltpu.make_async_copy(bases[x], basis_all.at[c, own_block], local.at[0]).start()

    for load in loads:
        load.start()
    own_basis = pltpu.make_async_copy(basis_query, basis_all.at[c, own_block], local.at[0])

    def basis_hop(source, slot, owner):
        block = basis_all.at[c, piece(source, owner), span_of(slot, rank)]
        return remote(
            block, block, ap_s.at[source, slot], ap_r.at[source, slot], rep=targets[slot]
        )

    def weight_fs(x, source, target):
        return remote(
            weights[x][0].at[own_part],
            weights[x][1].at[piece(source, r)],
            ez_s.at[x, target],
            ez_r.at[x, source],
            fs=target,
        )

    def weight_hop(x, source, slot, owner):
        block = weights[x][1].at[piece(source, owner), span_of(slot, weights[x][1].shape[1])]
        return remote(
            block, block, ep_s.at[x, source, slot], ep_r.at[x, source, slot], rep=targets[slot]
        )

    for load in loads[:2]:
        load.wait()
    wide_query[...] = loaded_query[...].astype(jnp.bfloat16)
    wide_key[...] = loaded_key[...].astype(jnp.bfloat16)

    def spread_basis(i):
        source = behind(i)
        basis_fs(0, source, source).wait_recv()
        for slot in (0, 1):
            basis_hop(source, slot, owners[slot]).start()

    each(1, fs, spread_basis)

    own_copies = [
        pltpu.make_async_copy(wide_query, weight_query_all.at[own_block], local.at[1]),
        pltpu.make_async_copy(wide_key, weight_key_all.at[own_block], local.at[2]),
    ]
    for copy in own_copies:
        copy.start()

    def start_weight(i):
        weight_fs(0, f, ahead(i)).start()
        weight_fs(1, f, ahead(i)).start()

    each(1, fs, start_weight)

    def relay_basis(i):
        source = behind(i)
        for slot in (0, 1):
            basis_hop(source, slot, senders[slot]).wait_recv()
            basis_hop(source, slot + 2, owners[slot + 2]).start()

    def all_basis(i):
        for slot in (2, 3):
            basis_hop(behind(i), slot, senders[slot]).wait_recv()

    each(1, fs, relay_basis)
    each(1, fs, all_basis)
    own_basis.wait()
    for load in loads[2:]:
        load.wait()

    for t in range(0, tokens, LANES):
        value = jnp.dot(
            inputs[t : t + LANES, :], basis_all[c], preferred_element_type=jnp.float32
        )
        factor[c, :, t : t + LANES] = value.T.astype(jnp.bfloat16)
    for u in range(units, per * rep):
        part_send[u] = jnp.zeros(part_send.shape[1:], jnp.bfloat16)
    factor_copy = remote(
        factor.at[c], factor.at[c], pair_s.at[0], pair_r.at[0], tp=1 - c
    )
    factor_back = remote(
        factor.at[1 - c], factor.at[1 - c], pair_s.at[0], pair_r.at[0], tp=1 - c
    )
    factor_copy.start()
    swap = remote(basis_all.at[c], basis_all.at[c], pair_s.at[1], pair_r.at[1], tp=1 - c)
    swap_back = remote(
        basis_all.at[1 - c], basis_all.at[1 - c], pair_s.at[1], pair_r.at[1], tp=1 - c
    )
    factor_back.wait_recv()
    swap.start()

    for x, cot in ((0, cot_query), (1, cot_key)):
        columns = cot.shape[1]
        width = 2 * LANES if columns % (2 * LANES) == 0 else LANES
        for n in range(0, columns, width):
            value = jnp.dot(
                factor[x], cot[:, n : n + width], preferred_element_type=jnp.float32
            ).astype(jnp.bfloat16)
            for k in range(0, width, LANES):
                part_send[x * query_units + (n + k) // LANES] = value[:, k : k + LANES]

    def group(owner):
        return pl.ds(owner * per, per)

    def part_rep(source, target):
        return remote(
            part_send.at[group(target)],
            part_recv.at[source],
            bp_s.at[target],
            bp_r.at[source],
            rep=target,
        )

    each(1, rep, lambda j: part_rep(r, beside(j)).start())
    part_recv[r] = part_send[group(r)]
    each(1, rep, lambda j: part_rep(beside(j), beside(j)).wait_recv())
    for p in range(per):
        value = part_recv[0, p].astype(jnp.float32)
        for q in range(1, rep):
            value = value + part_recv[q, p].astype(jnp.float32)
        slab[p] = value.astype(jnp.bfloat16)

    def slab_fs(source, target):
        return remote(
            slab.at[:, low_rows(target)],
            slab_recv.at[source],
            bz_s.at[target],
            bz_r.at[source],
            fs=target,
        )

    each(1, fs, lambda i: slab_fs(f, ahead(i)).start())

    def spread_weight(i):
        source = behind(i)
        for x in range(2):
            weight_fs(x, source, source).wait_recv()
            for slot in (0, 1):
                weight_hop(x, source, slot, owners[slot]).start()

    def relay_weight(i):
        source = behind(i)
        for slot in (0, 1):
            for x in range(2):
                weight_hop(x, source, slot, senders[slot]).wait_recv()
                weight_hop(x, source, slot + 2, owners[slot + 2]).start()

    spread_weight(1)
    slab_recv[f] = slab[:, low_rows(f), :]
    each(1, fs, lambda i: slab_fs(behind(i), behind(i)).wait_recv())
    for p in range(per):
        value = slab_recv[0, p].astype(jnp.float32)
        for q in range(1, fs):
            value = value + slab_recv[q, p].astype(jnp.float32)
        low_all[r * per + p] = value.astype(jnp.bfloat16)

    def low_rep(owner, target):
        block = low_all.at[group(owner)]
        return remote(block, block, lp_s.at[target], lp_r.at[owner], rep=target)

    each(1, rep, lambda j: low_rep(r, beside(j)).start())
    each(1, rep, lambda j: low_rep(beside(j), beside(j)).wait_recv())

    for x, moments, direction, low_out in (
        (0, moments_query, dir_query, low_query),
        (1, moments_key, dir_key, low_key),
    ):
        total = jnp.zeros((8, LANES), jnp.float32)
        for n in range(0, moments.shape[2], LANES):
            span = slice(n, n + LANES)
            low = low_all[x * query_units + n // LANES].astype(jnp.float32)
            low_out[:, span] = low
            first = 0.9 * moments[0, :, span] + 0.1 * low
            second = 0.95 * moments[1, :, span] + 0.05 * low * low
            normed = first / (jnp.sqrt(second) + 1e-08)
            direction[low_rows(f), span] = normed.astype(jnp.bfloat16)
            total = total + jnp.sum((normed * normed).reshape(rows // 8, 8, LANES), axis=0)
        squares[f, x] = total

    directions = (dir_query, dir_key)

    right, left = ahead(1), behind(1)

    def move_right(x, source):
        block = directions[x].at[low_rows(source)]
        return remote(block, block, dr_s.at[x, source], dz_r.at[x, source], fs=right)

    def move_left(x, source):
        block = directions[x].at[low_rows(source)]
        return remote(block, block, dl_s.at[x, source], dz_r.at[x, source], fs=left)

    def squares_fs(source, target):
        block = squares.at[source]
        return remote(block, block, qz_s.at[target], qz_r.at[source], fs=target)

    each(1, fs, lambda i: squares_fs(f, ahead(i)).start())

    @pl.when(f + 1 < fs)
    def start_right():
        for x in range(2):
            move_right(x, f).start()

    @pl.when(f > 0)
    def start_left():
        for x in range(2):
            move_left(x, f).start()

    each(2, fs, spread_weight)

    def relay_direction(k):
        @pl.when(f - k >= 0)
        def from_left():
            for x in range(2):
                move_right(x, f - k).wait_recv()

                @pl.when(f + 1 < fs)
                def onward():
                    move_right(x, f - k).start()

        @pl.when(f + k < fs)
        def from_right():
            for x in range(2):
                move_left(x, f + k).wait_recv()

                @pl.when(f > 0)
                def onward():
                    move_left(x, f + k).start()

    def relay_both(k):
        relay_weight(k)
        relay_direction(k)

    each(1, fs, relay_both)

    each(1, fs, lambda i: squares_fs(behind(i), behind(i)).wait_recv())
    total = squares[0]
    for q in range(1, fs):
        total = total + squares[q]
    pair[c] = total
    total_copy = remote(pair.at[c], pair.at[c], pair_s.at[2], pair_r.at[2], tp=1 - c)
    total_back = remote(pair.at[1 - c], pair.at[1 - c], pair_s.at[2], pair_r.at[2], tp=1 - c)
    total_copy.start()
    total_back.wait_recv()
    totals[...] = pair[0] + pair[1]

    def end_fs(i):
        source, target = behind(i), ahead(i)
        for x in range(2):
            for slot in (2, 3):
                weight_hop(x, source, slot, senders[slot]).wait_recv()
            for slot in range(4):
                weight_hop(x, source, slot, owners[slot]).wait_send()
            weight_fs(x, f, target).wait_send()
        for slot in range(4):
            basis_hop(source, slot, owners[slot]).wait_send()
        basis_fs(0, f, target).wait_send()
        slab_fs(f, target).wait_send()
        squares_fs(f, target).wait_send()

    def end_direction(k):
        @pl.when((f - k >= 0) & (f + 1 < fs))
        def end_right():
            for x in range(2):
                move_right(x, f - k).wait_send()

        @pl.when((f + k < fs) & (f > 0))
        def end_left():
            for x in range(2):
                move_left(x, f + k).wait_send()

    def end_rep(j):
        part_rep(r, beside(j)).wait_send()
        low_rep(r, beside(j)).wait_send()

    each(1, fs, end_fs)
    each(0, fs, end_direction)
    each(1, rep, end_rep)
    swap_back.wait_recv()
    factor_copy.wait_send()
    swap.wait_send()
    total_copy.wait_send()
    for copy in own_copies:
        copy.wait()


def apply(
    count_query,
    count_key,
    totals,
    dir_query,
    dir_key,
    low_query,
    low_key,
    moments_query,
    moments_key,
    basis_all,
    weight_query_all,
    weight_key_all,
    basis_query,
    basis_key,
    weight_query,
    weight_key,
    step_query,
    step_key,
    new_weight_query,
    new_weight_key,
    copy_query,
    copy_key,
    new_moments_query,
    new_moments_key,
):
    parts = (
        (count_query, dir_query, weight_query_all, basis_query, weight_query),
        (count_key, dir_key, weight_key_all, basis_key, weight_key),
    )
    outs = (
        (step_query, new_weight_query, copy_query),
        (step_key, new_weight_key, copy_key),
    )
    for x in range(2):
        count, direction, weight_all, basis, weight = parts[x]
        step_out, new_weight_out, copy_out = outs[x]
        scale = lax.rsqrt(jnp.sum(totals[x], keepdims=True) / count + 1e-06)
        step = scale * jnp.dot(basis[...], direction[...], preferred_element_type=jnp.float32)
        step_out[...] = step
        new_weight_out[...] = weight[...] - 0.02 * step
        whole = scale * jnp.dot(
            basis_all[x], direction[...], preferred_element_type=jnp.float32
        )
        copy_out[...] = (weight_all[...].astype(jnp.float32) - 0.02 * whole).astype(jnp.bfloat16)

    @pl.when(pl.program_id(0) == 0)
    def moments_once():
        for moments, low_ref, out in (
            (moments_query, low_query, new_moments_query),
            (moments_key, low_key, new_moments_key),
        ):
            low = low_ref[...]
            out[0] = 0.9 * moments[0] + 0.1 * low
            out[1] = 0.95 * moments[1] + 0.05 * low * low


def on_device(
    inputs,
    cot_query,
    cot_key,
    basis_query,
    basis_key,
    weight_query,
    weight_key,
    moments_query,
    moments_key,
):
    fs, rep, tp = lax.axis_size("fs"), lax.axis_size("rep"), lax.axis_size("tp")
    assert tp == 2 and rep == 4
    height, rank = basis_query.shape
    rows = rank // fs
    tokens = inputs.shape[0]
    query_cols, key_cols = cot_query.shape[1], cot_key.shape[1]
    per = -(-((query_cols + key_cols) // LANES) // rep)
    vmem = pl.BlockSpec(memory_space=pltpu.VMEM)
    hbm = pl.BlockSpec(memory_space=pl.ANY)
    bf16, f32 = jnp.bfloat16, jnp.float32
    dma = pltpu.SemaphoreType.DMA
    shape = jax.ShapeDtypeStruct
    (
        basis_all,
        weight_query_all,
        weight_key_all,
        dir_query,
        dir_key,
        low_query,
        low_key,
        totals,
    ) = pl.pallas_call(
        functools.partial(exchange, fs, rep),
        out_shape=(
            shape((2, height * fs, rank), bf16),
            shape((height * fs, query_cols), bf16),
            shape((height * fs, key_cols), bf16),
            shape((rank, query_cols), bf16),
            shape((rank, key_cols), bf16),
            shape((rows, query_cols), f32),
            shape((rows, key_cols), f32),
            shape((2, 8, LANES), f32),
        ),
        in_specs=[pl.BlockSpec(memory_space=pltpu.HBM)] * 9,
        out_specs=(vmem, hbm, hbm, vmem, vmem, vmem, vmem, vmem),
        scratch_shapes=[
            pltpu.VMEM((tokens, inputs.shape[1]), bf16),
            pltpu.VMEM((tokens, query_cols), bf16),
            pltpu.VMEM((tokens, key_cols), bf16),
            pltpu.VMEM((2, rows, query_cols), f32),
            pltpu.VMEM((2, rows, key_cols), f32),
            pltpu.VMEM((height, query_cols), f32),
            pltpu.VMEM((height, key_cols), f32),
            pltpu.VMEM((height, query_cols), bf16),
            pltpu.VMEM((height, key_cols), bf16),
            pltpu.VMEM((2, rank, tokens), bf16),
            pltpu.VMEM((per * rep, rank, LANES), bf16),
            pltpu.VMEM((rep, per, rank, LANES), bf16),
            pltpu.VMEM((per, rank, LANES), bf16),
            pltpu.VMEM((fs, per, rows, LANES), bf16),
            pltpu.VMEM((per * rep, rows, LANES), bf16),
            pltpu.VMEM((fs, 2, 8, LANES), f32),
            pltpu.VMEM((2, 2, 8, LANES), f32),
            dma((fs,)),
            dma((fs,)),
            dma((fs, rep)),
            dma((fs, rep)),
            dma((2, fs)),
            dma((2, fs)),
            dma((2, fs, rep)),
            dma((2, fs, rep)),
            dma((rep,)),
            dma((rep,)),
            dma((fs,)),
            dma((fs,)),
            dma((rep,)),
            dma((rep,)),
            dma((2, fs)),
            dma((2, fs)),
            dma((2, fs)),
            dma((fs,)),
            dma((fs,)),
            dma((3,)),
            dma((3,)),
            dma((10,)),
        ],
        compiler_params=pltpu.CompilerParams(
            collective_id=0, has_side_effects=True, vmem_limit_bytes=32 * 1024 * 1024
        ),
    )(
        *(
            pltpu.with_memory_space_constraint(operand, pltpu.HBM)
            for operand in (
                inputs,
                cot_query,
                cot_key,
                basis_query,
                basis_key,
                weight_query,
                weight_key,
                moments_query,
                moments_key,
            )
        )
    )

    steps = min(8, height // 16)
    tall, short = height * fs // steps, height // steps

    def fixed(*dims):
        return pl.BlockSpec(dims, lambda i: (0,) * len(dims))

    def banded(*dims):
        return pl.BlockSpec(dims, lambda i: (i, 0))

    owned = tuple(
        shape((height, columns), f32) for columns in (query_cols, key_cols, query_cols, key_cols)
    )
    owned_specs = tuple(
        banded(short, columns) for columns in (query_cols, key_cols, query_cols, key_cols)
    )
    return pl.pallas_call(
        functools.partial(
            apply, float(rank * query_cols * tp), float(rank * key_cols * tp)
        ),
        grid=(steps,),
        out_shape=owned
        + (
            shape((height * fs, query_cols), bf16),
            shape((height * fs, key_cols), bf16),
            shape((2, rows, query_cols), f32),
            shape((2, rows, key_cols), f32),
        ),
        in_specs=[
            fixed(2, 8, LANES),
            fixed(rank, query_cols),
            fixed(rank, key_cols),
            fixed(rows, query_cols),
            fixed(rows, key_cols),
            fixed(2, rows, query_cols),
            fixed(2, rows, key_cols),
            pl.BlockSpec((2, tall, rank), lambda i: (0, i, 0)),
            banded(tall, query_cols),
            banded(tall, key_cols),
            banded(short, rank),
            banded(short, rank),
            banded(short, query_cols),
            banded(short, key_cols),
        ],
        out_specs=owned_specs
        + (
            banded(tall, query_cols),
            banded(tall, key_cols),
            fixed(2, rows, query_cols),
            fixed(2, rows, key_cols),
        ),
        compiler_params=pltpu.CompilerParams(
            dimension_semantics=("arbitrary",), vmem_limit_bytes=32 * 1024 * 1024
        ),
    )(
        totals,
        dir_query,
        dir_key,
        low_query,
        low_key,
        moments_query,
        moments_key,
        basis_all,
        weight_query_all,
        weight_key_all,
        basis_query,
        basis_key,
        weight_query,
        weight_key,
    )


def solution(mesh):
    in_specs = (
        P(("fs", "rep"), None),
        P(("fs", "rep"), "tp"),
        P(("fs", "rep"), "tp"),
        P("fs", None),
        P("fs", None),
        P("fs", "tp"),
        P("fs", "tp"),
        P(None, "fs", "tp"),
        P(None, "fs", "tp"),
    )
    out_specs = (
        P("fs", "tp"),
        P("fs", "tp"),
        P("fs", "tp"),
        P("fs", "tp"),
        P(None, "tp"),
        P(None, "tp"),
        P(None, "fs", "tp"),
        P(None, "fs", "tp"),
    )
    return jax.shard_map(
        on_device, mesh=mesh, in_specs=in_specs, out_specs=out_specs, check_vma=False
    )
```

profile of v0, /device:TPU:0, one launch (start us, length us, event | category | flops | bytes accessed | tf_op | source)
XLA Modules:
  0.0 100.5 jit_solution(11985207674569250137)
XLA Ops:
  0.6 0.0 copy-start.5
  0.6 0.0 copy-start.1
  0.7 0.0 copy-start.4
  0.7 0.0 copy-start
  0.7 0.0 copy-start.3
  0.7 0.0 copy-start.2
  0.7 91.1 %shard_map.152 = (bf16[2,2048,512]{2,1,0:T(8,128)(2,1)S(1)}, bf16[2048,1024]{1,0:T(8,128)(2,1)S(1)}, bf16[2048,256]{1,0:T(8,128)(2,1)S(1)}, bf16[512,1024]{1,0:T...) custom-call(bf16[256,2048]{1,0:T(8,128)(2,1)} %inputs_far.1, ...), custom_call_target="tpu_custom_call" | custom-call | tf_op jit(solution)/shard_map/pallas_call | solution.py:547
  91.8 0.0 copy-done.5
  91.8 0.0 copy-done.1
  91.8 0.0 copy-done.4
  91.8 0.0 copy-done
  91.9 0.0 copy-done.3
  91.9 0.0 copy-done.2
  91.9 8.7 %shard_map.153 = (f32[512,1024]{1,0:T(8,128)}, f32[512,256]{1,0:T(8,128)}, f32[512,1024]{1,0:T(8,128)}, f32[512,256]{1,0:T(8,128)}, bf16[2048,1024]{1,0:T(8,128)...) custom-call(f32[2,8,128]{2,1,0:T(8,128)S(1)} %get-tuple-element.16.totals, ...), custom_call_target="tpu_custom_call" | custom-call | tf_op jit(solution)/shard_map/pallas_call | solution.py:637
Async XLA Ops:
  0.6 91.2 %copy-start.5 = (f32[2,128,256]{2,1,0:T(8,128)S(1)}, f32[2,128,256]{2,1,0:T(8,128)}, u32[]{:S(2)}) copy-start(f32[2,128,256]{2,1,0:T(8,128)} %moments_key.1) | copy-start | bytes 786436
  0.6 91.2 %copy-start.1 = (f32[2,128,1024]{2,1,0:T(8,128)S(1)}, f32[2,128,1024]{2,1,0:T(8,128)}, u32[]{:S(2)}) copy-start(f32[2,128,1024]{2,1,0:T(8,128)} %moments_query.1) | copy-start | bytes 3145732
  0.7 91.2 %copy-start.4 = (f32[512,256]{1,0:T(8,128)S(1)}, f32[512,256]{1,0:T(8,128)}, u32[]{:S(2)}) copy-start(f32[512,256]{1,0:T(8,128)} %weight_key.1) | copy-start | bytes 1572868
  0.7 91.2 %copy-start = (f32[512,1024]{1,0:T(8,128)S(1)}, f32[512,1024]{1,0:T(8,128)}, u32[]{:S(2)}) copy-start(f32[512,1024]{1,0:T(8,128)} %weight_query.1) | copy-start | bytes 6291460
  0.7 91.2 %copy-start.3 = (bf16[512,512]{1,0:T(8,128)(2,1)S(1)}, bf16[512,512]{1,0:T(8,128)(2,1)}, u32[]{:S(2)}) copy-start(bf16[512,512]{1,0:T(8,128)(2,1)} %basis_key.3) | copy-start | bytes 1572868
  0.7 91.2 %copy-start.2 = (bf16[512,512]{1,0:T(8,128)(2,1)S(1)}, bf16[512,512]{1,0:T(8,128)(2,1)}, u32[]{:S(2)}) copy-start(bf16[512,512]{1,0:T(8,128)(2,1)} %basis_query.3) | copy-start | bytes 1572868
where the time goes:
time: 101 us
  Pallas kernels  99.8 us (99%)
    pallas_call x1, Pallas kernels, on_device(): pl.pallas_call(functools.partial(exchange, fs, rep), out_shape=(shape((2,...  91.1 us
    pallas_call x1, Pallas kernels, on_device(): pl.pallas_call(functools.partial(apply, float(rank * query_cols * tp), fl...  8.65 us

commit v1 on v0

--- a/solution.py
+++ b/solution.py
@@ -455,6 +455,550 @@
         copy.wait()
 
 
+def exchange_grid(
+    fs,
+    rep,
+    inputs_far,
+    cot_query_far,
+    cot_key_far,
+    basis_query,
+    basis_key,
+    full_query,
+    full_key,
+    moments_query_far,
+    moments_key_far,
+    basis_all,
+    weight_query_all,
+    weight_key_all,
+    dir_query,
+    dir_key,
+    low_query,
+    low_key,
+    totals,
+    inputs,
+    cot_query,
+    cot_key,
+    moments_query,
+    moments_key,
+    loaded_query,
+    loaded_key,
+    factor,
+    part,
+    got_first,
+    pair_sum,
+    got_second,
+    slab,
+    slab_recv,
+    low_all,
+    part_squares,
+    squares,
+    pair,
+    az_s,
+    az_r,
+    ap_s,
+    ap_r,
+    wz_s,
+    wz_r,
+    wp_s,
+    wp_r,
+    kz_s,
+    kz_r,
+    h1_s,
+    h1_r,
+    h2_s,
+    h2_r,
+    bz_s,
+    bz_r,
+    lp_s,
+    lp_r,
+    dz_s,
+    dz_r,
+    dp_s,
+    dp_r,
+    qz_s,
+    qz_r,
+    pair_s,
+    pair_r,
+    local,
+):
+    f, r, c = lax.axis_index("fs"), lax.axis_index("rep"), lax.axis_index("tp")
+    height, rank = basis_query.shape
+    quarter = height // rep
+    rows = rank // fs
+    own = rows // rep
+    tokens = inputs.shape[0]
+    query_units = cot_query.shape[1] // LANES
+    units = query_units + cot_key.shape[1] // LANES
+    streams = ((0, units // 2), (units // 2, units // 2))
+    f32, bf16 = jnp.float32, jnp.bfloat16
+
+    near = r + 1 - 2 * lax.rem(r, 2)
+    far = r + 2 - 4 * (r // 2)
+    across = 3 - r
+    pending = []
+
+    def when(conds, body):
+        if not conds:
+            body()
+            return
+        test = conds[0]
+        for cond in conds[1:]:
+            test = test & cond
+        pl.when(test)(body)
+
+    def send(make, *conds):
+        when(conds, lambda: make().start())
+        pending.append((make, conds))
+
+    def receive(make, *conds):
+        when(conds, lambda: make().wait_recv())
+
+    def sources(d):
+        return ((f - d, f >= d), (f + d, f + d < fs))
+
+    def beside(j):
+        return lax.rem(r + j, rep)
+
+    def rows_of(start, size):
+        return pl.ds(pl.multiple_of(start, size), size)
+
+    chunks = 2
+    chunk = quarter // chunks
+
+    def piece(source, owner, k):
+        return rows_of(source * height + owner * quarter + k * chunk, chunk)
+
+    mirror = f // (fs // 2)
+    place_in_half = f + mirror * (fs - 1 - 2 * f)
+
+    def other(n):
+        low_side = n - 1 + (n + fs - 1 - place_in_half) // fs
+        return low_side + mirror * (fs - 1 - 2 * low_side)
+
+    own_block = rows_of(f * height, height)
+
+    loads = [
+        pltpu.make_async_copy(source, target, local.at[1 + n])
+        for n, (source, target) in enumerate(
+            (
+                (full_query, loaded_query),
+                (full_key, loaded_key),
+                (inputs_far, inputs),
+                (cot_query_far, cot_query),
+                (cot_key_far, cot_key),
+                (moments_query_far, moments_query),
+                (moments_key_far, moments_key),
+            )
+        )
+    ]
+    barrier = pltpu.get_barrier_semaphore()
+    for i in range(1, fs):
+        pl.semaphore_signal(
+            barrier, inc=1, device_id={"fs": lax.rem(f + i, fs)}, device_id_type=MESH
+        )
+    for mate in (near, far):
+        pl.semaphore_signal(barrier, inc=1, device_id={"rep": mate}, device_id_type=MESH)
+    pl.semaphore_signal(barrier, inc=1, device_id={"tp": 1 - c}, device_id_type=MESH)
+    pl.semaphore_wait(barrier, fs + 2)
+
+    bases = (basis_query, basis_key)
+
+    def basis_z(source, up, k):
+        block = basis_all.at[c, piece(source, r, k)]
+        return remote(
+            block, block, az_s.at[1 - up, source, k], az_r.at[source, k], fs=f + 2 * up - 1
+        )
+
+    def basis_start(x, up, k):
+        return remote(
+            bases[x].at[rows_of(r * quarter + k * chunk, chunk)],
+            basis_all.at[c, piece(f, r, k)],
+            az_s.at[1 - up, f, k],
+            az_r.at[f, k],
+            fs=f + 2 * up - 1,
+        )
+
+    ways = ((1, f + 1 < fs), (0, f > 0))
+    for x in range(2):
+
+        @pl.when(c == x)
+        def start_basis():
+            for k in range(chunks):
+                for up, there in ways:
+                    pl.when(there)(lambda: basis_start(x, up, k).start())
+            pltpu.make_async_copy(bases[x], basis_all.at[c, own_block], local.at[0]).start()
+
+    for k in range(chunks):
+        for up, there in ways:
+            pending.append((functools.partial(basis_z, f, up, k), (there,)))
+    for load in loads:
+        load.start()
+    own_basis = pltpu.make_async_copy(basis_query, basis_all.at[c, own_block], local.at[0])
+
+    def hop_span(slot, width):
+        return (pl.ds(0, width), pl.ds(0, width), pl.ds(0, width // 2), pl.ds(width // 2, width // 2))[slot]
+
+    targets = (near, far, far, near)
+    sent = (r, r, near, far)
+    arriving = (near, far, across, across)
+
+    def basis_hop(k, source, slot, owner):
+        block = basis_all.at[c, piece(source, owner, k), hop_span(slot, rank)]
+        return remote(
+            block, block, ap_s.at[source, slot, k], ap_r.at[source, slot, k], rep=targets[slot]
+        )
+
+    def weight_hop(k, source, slot, owner):
+        width = weight_query_all.shape[1]
+        block = weight_query_all.at[piece(source, owner, k), hop_span(slot, width)]
+        return remote(
+            block, block, wp_s.at[source, slot, k], wp_r.at[source, slot, k], rep=targets[slot]
+        )
+
+    def spread(hop, source, *there):
+        for slot in (0, 1):
+            send(functools.partial(hop, source, slot, sent[slot]), *there)
+
+    def relay(hop, source, *there):
+        for slot in (0, 1):
+            receive(functools.partial(hop, source, slot, arriving[slot]), *there)
+            send(functools.partial(hop, source, slot + 2, sent[slot + 2]), *there)
+
+    def finish(hop, source, *there):
+        for slot in (2, 3):
+            receive(functools.partial(hop, source, slot, arriving[slot]), *there)
+
+    def query_z(source, up, k):
+        block = weight_query_all.at[piece(source, r, k)]
+        return remote(
+            block, block, wz_s.at[1 - up, source, k], wz_r.at[source, k], fs=f + 2 * up - 1
+        )
+
+    def key_z(source, up, k):
+        block = weight_key_all.at[rows_of(source * height + k * (height // chunks), height // chunks)]
+        return remote(
+            block, block, kz_s.at[1 - up, source, k], kz_r.at[source, k], fs=f + 2 * up - 1
+        )
+
+    def launch(line):
+        for k in range(chunks):
+            for up, there in ways:
+                send(functools.partial(line, f, up, k), there)
+
+    def onward(line, d, k):
+        below, above = f - d, f + d
+        receive(functools.partial(line, below, 1, k), f >= d)
+        if d + 1 < fs:
+            send(functools.partial(line, below, 1, k), f >= d, f + 1 < fs)
+        receive(functools.partial(line, above, 0, k), f + d < fs)
+        if d + 1 < fs:
+            send(functools.partial(line, above, 0, k), f + d < fs, f > 0)
+
+    def onward_all(line, d):
+        for k in range(chunks):
+            onward(line, d, k)
+
+    for load in loads[:2]:
+        load.wait()
+    weight_query_all[own_block, :] = loaded_query[...].astype(bf16)
+    weight_key_all[own_block, :] = loaded_key[...].astype(bf16)
+
+    steps = [(d, k) for d in range(1, fs) for k in range(chunks)]
+    for n, (d, k) in enumerate(steps):
+        onward(basis_z, d, k)
+        for source, there in sources(d):
+            spread(functools.partial(basis_hop, k), source, there)
+        if (d, k) == (max(fs - 2, 1), chunks - 1):
+            launch(query_z)
+            launch(key_z)
+        if n >= chunks:
+            before, j = steps[n - chunks]
+            for source, there in sources(before):
+                relay(functools.partial(basis_hop, j), source, there)
+    for d, k in steps[-chunks:]:
+        for source, there in sources(d):
+            relay(functools.partial(basis_hop, k), source, there)
+    onward_all(query_z, 1)
+    spread(functools.partial(weight_hop, 0), other(1))
+    for d, k in steps:
+        for source, there in sources(d):
+            finish(functools.partial(basis_hop, k), source, there)
+    own_basis.wait()
+    for load in loads[2:]:
+        load.wait()
+
+    for t in range(0, tokens, LANES):
+        value = jnp.dot(inputs[t : t + LANES, :], basis_all[c], preferred_element_type=f32)
+        factor[c, :, t : t + LANES] = value.T.astype(bf16)
+
+    def partner(block, back, n):
+        return (
+            remote(block, block, pair_s.at[n], pair_r.at[n], tp=1 - c),
+            remote(back, back, pair_s.at[n], pair_r.at[n], tp=1 - c),
+        )
+
+    factor_copy, factor_back = partner(factor.at[c], factor.at[1 - c], 0)
+    swap, swap_back = partner(basis_all.at[c], basis_all.at[1 - c], 1)
+    factor_copy.start()
+    factor_back.wait_recv()
+    swap.start()
+
+    for x, cot in ((0, cot_query), (1, cot_key)):
+        columns = cot.shape[1]
+        width = 2 * LANES if columns % (2 * LANES) == 0 else LANES
+        for n in range(0, columns, width):
+            value = jnp.dot(
+                factor[x], cot[:, n : n + width], preferred_element_type=f32
+            ).astype(bf16)
+            for k in range(0, width, LANES):
+                for q in range(rep):
+                    for s in range(fs):
+                        part[x * query_units + (n + k) // LANES, q, s * own : (s + 1) * own] = value[
+                            s * rows + q * own : s * rows + (q + 1) * own, k : k + LANES
+                        ]
+
+    half = rows // 2
+    spans = (slice(0, half), slice(half, rows))
+    mates = ((near, far), (far, near))
+
+    def columns_of(g):
+        return pl.ds(streams[g][0], streams[g][1])
+
+    def first_hop(h, g, w):
+        owner = (across, mates[h][0])[w]
+        return remote(
+            part.at[columns_of(g), owner, pl.ds(h * half, half)],
+            got_first.at[h, w, columns_of(g)],
+            h1_s.at[h, w, g],
+            h1_r.at[h, w, g],
+            rep=mates[h][0],
+        )
+
+    def second_hop(h, g):
+        return remote(
+            pair_sum.at[h, columns_of(g)],
+            got_second.at[h, columns_of(g)],
+            h2_s.at[h, g],
+            h2_r.at[h, g],
+            rep=mates[h][1],
+        )
+
+    def start_first(g, w):
+        for h in range(2):
+            send(functools.partial(first_hop, h, g, w))
+
+    def start_second(g):
+        for h in range(2):
+            receive(functools.partial(first_hop, h, g, 0))
+            for u in range(streams[g][0], sum(streams[g])):
+                pair_sum[h, u] = (
+                    part[u, mates[h][1], spans[h]].astype(f32) + got_first[h, 0, u].astype(f32)
+                ).astype(bf16)
+            send(functools.partial(second_hop, h, g))
+
+    def slab_z(g, source, target):
+        return remote(
+            slab.at[columns_of(g), rows_of(target * own, own)],
+            slab_recv.at[source, columns_of(g)],
+            bz_s.at[g, target],
+            bz_r.at[g, source],
+            fs=target,
+        )
+
+    def end_rep(g):
+        for h in range(2):
+            receive(functools.partial(first_hop, h, g, 1))
+            receive(functools.partial(second_hop, h, g))
+            for u in range(streams[g][0], sum(streams[g])):
+                slab[u, spans[h]] = (
+                    part[u, r, spans[h]].astype(f32)
+                    + got_first[h, 1, u].astype(f32)
+                    + got_second[h, u].astype(f32)
+                ).astype(bf16)
+        for d in range(fs - 1, 0, -1):
+            for target, there in sources(d):
+                send(functools.partial(slab_z, g, f, target), there)
+        for u in range(streams[g][0], sum(streams[g])):
+            slab_recv[f, u] = slab[u, rows_of(f * own, own)]
+
+    start_first(0, 0)
+    start_first(0, 1)
+    start_first(1, 0)
+    start_second(0)
+    start_first(1, 1)
+    start_second(1)
+    for k in range(1, chunks):
+        spread(functools.partial(weight_hop, k), other(1))
+    end_rep(0)
+    end_rep(1)
+    onward_all(query_z, 2)
+    for k in range(chunks):
+        spread(functools.partial(weight_hop, k), other(2))
+
+    directions, lows = (dir_query, dir_key), (low_query, low_key)
+    moments = (moments_query, moments_key)
+
+    def place(u):
+        x = 0 if u < query_units else 1
+        n = (u - x * query_units) * LANES
+        return x, slice(n, n + LANES)
+
+    def pieces(g):
+        first, last = streams[g][0], sum(streams[g])
+        found = []
+        if first < query_units:
+            found.append((0, first * LANES, (min(last, query_units) - first) * LANES))
+        if last > query_units:
+            start = max(first, query_units)
+            found.append((1, (start - query_units) * LANES, (last - start) * LANES))
+        return found
+
+    def dir_rows(source, owner):
+        return rows_of(source * rows + owner * own, own)
+
+    def update(g, owner):
+        sums = [jnp.zeros((8, LANES), f32), jnp.zeros((8, LANES), f32)]
+        mine = rows_of(owner * own, own)
+        for u in range(streams[g][0], sum(streams[g])):
+            x, span = place(u)
+            low = low_all[owner, u].astype(f32)
+            lows[x][mine, span] = low
+            first = 0.9 * moments[x][0, mine, span] + 0.1 * low
+            second = 0.95 * moments[x][1, mine, span] + 0.05 * low * low
+            normed = first / (jnp.sqrt(second) + 1e-08)
+            directions[x][dir_rows(f, owner), span] = normed.astype(bf16)
+            sums[x] = sums[x] + jnp.sum((normed * normed).reshape(own // 8, 8, LANES), axis=0)
+        for x in range(2):
+            part_squares[owner, g, x] = sums[x]
+
+    def low_hop(g, slot, owner):
+        block = low_all.at[owner, columns_of(g)]
+        return remote(block, block, lp_s.at[slot, g], lp_r.at[slot, g], rep=targets[slot])
+
+    def dir_z(g, n, source, target):
+        x, start, size = pieces(g)[n]
+        block = directions[x].at[dir_rows(source, r), pl.ds(start, size)]
+        return remote(block, block, dz_s.at[g, n, target], dz_r.at[g, n, source], fs=target)
+
+    def dir_hop(g, n, slot, source, owner):
+        x, start, size = pieces(g)[n]
+        block = directions[x].at[dir_rows(source, owner), pl.ds(start, size)]
+        return remote(
+            block,
+            block,
+            dp_s.at[g, n, slot, source],
+            dp_r.at[g, n, slot, source],
+            rep=targets[slot],
+        )
+
+    def end_fs(g):
+        for d in range(1, fs):
+            for source, there in sources(d):
+                receive(functools.partial(slab_z, g, source, source), there)
+        for u in range(streams[g][0], sum(streams[g])):
+            value = slab_recv[0, u].astype(f32)
+            for q in range(1, fs):
+                value = value + slab_recv[q, u].astype(f32)
+            low_all[r, u] = value.astype(bf16)
+        for slot in (0, 1):
+            send(functools.partial(low_hop, g, slot, r))
+        update(g, r)
+        for d in range(fs - 1, 0, -1):
+            for target, there in sources(d):
+                for n in range(len(pieces(g))):
+                    send(functools.partial(dir_z, g, n, f, target), there)
+
+    end_fs(0)
+    end_fs(1)
+
+    def spread_dir(g, d):
+        for source, there in sources(d):
+            for n in range(len(pieces(g))):
+                receive(functools.partial(dir_z, g, n, source, source), there)
+                for slot in (0, 1):
+                    send(functools.partial(dir_hop, g, n, slot, source, r), there)
+
+    def relay_dir(d):
+        for source, there in sources(d):
+            for g in range(2):
+                for n in range(len(pieces(g))):
+                    receive(functools.partial(dir_hop, g, n, g, source, arriving[g]), there)
+                    send(functools.partial(dir_hop, g, n, g + 2, source, sent[g + 2]), there)
+
+    def finish_dir(d):
+        for source, there in sources(d):
+            for g in range(2):
+                for n in range(len(pieces(g))):
+                    receive(functools.partial(dir_hop, g, n, 1 - g, source, arriving[1 - g]), there)
+                    receive(functools.partial(dir_hop, g, n, g + 2, source, across), there)
+
+    onward_all(key_z, 1)
+    for k in range(chunks):
+        relay(functools.partial(weight_hop, k), other(1))
+    for g in range(2):
+        receive(functools.partial(low_hop, g, g, arriving[g]))
+        send(functools.partial(low_hop, g, g + 2, sent[g + 2]))
+    spread_dir(0, 1)
+    spread_dir(1, 1)
+    for d in range(2, fs):
+        spread_dir(0, d)
+        spread_dir(1, d)
+        relay_dir(d - 1)
+    relay_dir(fs - 1)
+    for k in range(chunks):
+        relay(functools.partial(weight_hop, k), other(2))
+    for n in range(3, fs):
+        for k in range(chunks):
+            onward(query_z, n, k)
+            spread(functools.partial(weight_hop, k), other(n))
+    for d in range(2, fs - 1):
+        onward_all(key_z, d)
+    for g in range(2):
+        receive(functools.partial(low_hop, g, 1 - g, arriving[1 - g]))
+        receive(functools.partial(low_hop, g, g + 2, across))
+        for j in range(1, rep):
+            update(g, beside(j))
+    for x in range(2):
+        total = part_squares[0, 0, x] + part_squares[0, 1, x]
+        for q in range(1, rep):
+            total = total + (part_squares[q, 0, x] + part_squares[q, 1, x])
+        squares[f, x] = total
+
+    def squares_z(source, target):
+        block = squares.at[source]
+        return remote(block, block, qz_s.at[target], qz_r.at[source], fs=target)
+
+    for d in range(1, fs):
+        for target, there in sources(d):
+            send(functools.partial(squares_z, f, target), there)
+    for d in range(1, fs):
+        for source, there in sources(d):
+            receive(functools.partial(squares_z, source, source), there)
+    total = squares[0]
+    for q in range(1, fs):
+        total = total + squares[q]
+    pair[c] = total
+    total_copy, total_back = partner(pair.at[c], pair.at[1 - c], 2)
+    total_copy.start()
+
+    for d in range(1, fs):
+        finish_dir(d)
+    for n in range(3, fs):
+        for k in range(chunks):
+            relay(functools.partial(weight_hop, k), other(n))
+    onward_all(key_z, fs - 1)
+    for n in range(1, fs):
+        for k in range(chunks):
+            finish(functools.partial(weight_hop, k), other(n))
+    total_back.wait_recv()
+    totals[...] = pair[0] + pair[1]
+    for make, conds in pending:
+        when(conds, lambda: make().wait_send())
+    swap_back.wait_recv()
+    for copy in (factor_copy, swap, total_copy):
+        copy.wait_send()
+
+
 def apply(
     count_query,
     count_key,
@@ -535,30 +1079,69 @@
     bf16, f32 = jnp.bfloat16, jnp.float32
     dma = pltpu.SemaphoreType.DMA
     shape = jax.ShapeDtypeStruct
-    (
-        basis_all,
-        weight_query_all,
-        weight_key_all,
-        dir_query,
-        dir_key,
-        low_query,
-        low_key,
-        totals,
-    ) = pl.pallas_call(
-        functools.partial(exchange, fs, rep),
-        out_shape=(
-            shape((2, height * fs, rank), bf16),
-            shape((height * fs, query_cols), bf16),
-            shape((height * fs, key_cols), bf16),
-            shape((rank, query_cols), bf16),
-            shape((rank, key_cols), bf16),
-            shape((rows, query_cols), f32),
-            shape((rows, key_cols), f32),
-            shape((2, 8, LANES), f32),
-        ),
-        in_specs=[pl.BlockSpec(memory_space=pltpu.HBM)] * 9,
-        out_specs=(vmem, hbm, hbm, vmem, vmem, vmem, vmem, vmem),
-        scratch_shapes=[
+    out_shape = (
+        shape((2, height * fs, rank), bf16),
+        shape((height * fs, query_cols), bf16),
+        shape((height * fs, key_cols), bf16),
+        shape((rank, query_cols), bf16),
+        shape((rank, key_cols), bf16),
+        shape((rows, query_cols), f32),
+        shape((rows, key_cols), f32),
+        shape((2, 8, LANES), f32),
+    )
+    own, units = rows // rep, (query_cols + key_cols) // LANES
+    if own % 16 == 0 and fs % 2 == 0 and units % 2 == 0 and rows % rep == 0:
+        kernel, out_specs = exchange_grid, (vmem,) * 8
+        scratch = [
+            pltpu.VMEM((tokens, inputs.shape[1]), bf16),
+            pltpu.VMEM((tokens, query_cols), bf16),
+            pltpu.VMEM((tokens, key_cols), bf16),
+            pltpu.VMEM((2, rows, query_cols), f32),
+            pltpu.VMEM((2, rows, key_cols), f32),
+            pltpu.VMEM((height, query_cols), f32),
+            pltpu.VMEM((height, key_cols), f32),
+            pltpu.VMEM((2, rank, tokens), bf16),
+            pltpu.VMEM((units, rep, rows, LANES), bf16),
+            pltpu.VMEM((2, 2, units, rows // 2, LANES), bf16),
+            pltpu.VMEM((2, units, rows // 2, LANES), bf16),
+            pltpu.VMEM((2, units, rows // 2, LANES), bf16),
+            pltpu.VMEM((units, rows, LANES), bf16),
+            pltpu.VMEM((fs, units, own, LANES), bf16),
+            pltpu.VMEM((rep, units, own, LANES), bf16),
+            pltpu.VMEM((rep, 2, 2, 8, LANES), f32),
+            pltpu.VMEM((fs, 2, 8, LANES), f32),
+            pltpu.VMEM((2, 2, 8, LANES), f32),
+            dma((2, fs, 2)),
+            dma((fs, 2)),
+            dma((fs, rep, 2)),
+            dma((fs, rep, 2)),
+            dma((2, fs, 2)),
+            dma((fs, 2)),
+            dma((fs, rep, 2)),
+            dma((fs, rep, 2)),
+            dma((2, fs, 2)),
+            dma((fs, 2)),
+            dma((2, 2, 2)),
+            dma((2, 2, 2)),
+            dma((2, 2)),
+            dma((2, 2)),
+            dma((2, fs)),
+            dma((2, fs)),
+            dma((4, 2)),
+            dma((4, 2)),
+            dma((2, 2, fs)),
+            dma((2, 2, fs)),
+            dma((2, 2, 4, fs)),
+            dma((2, 2, 4, fs)),
+            dma((fs,)),
+            dma((fs,)),
+            dma((3,)),
+            dma((3,)),
+            dma((8,)),
+        ]
+    else:
+        kernel, out_specs = exchange, (vmem, hbm, hbm, vmem, vmem, vmem, vmem, vmem)
+        scratch = [
             pltpu.VMEM((tokens, inputs.shape[1]), bf16),
             pltpu.VMEM((tokens, query_cols), bf16),
             pltpu.VMEM((tokens, key_cols), bf16),
@@ -598,7 +1181,22 @@
             dma((3,)),
             dma((3,)),
             dma((10,)),
-        ],
+        ]
+    (
+        basis_all,
+        weight_query_all,
+        weight_key_all,
+        dir_query,
+        dir_key,
+        low_query,
+        low_key,
+        totals,
+    ) = pl.pallas_call(
+        functools.partial(kernel, fs, rep),
+        out_shape=out_shape,
+        in_specs=[pl.BlockSpec(memory_space=pltpu.HBM)] * 9,
+        out_specs=out_specs,
+        scratch_shapes=scratch,
         compiler_params=pltpu.CompilerParams(
             collective_id=0, has_side_effects=True, vmem_limit_bytes=32 * 1024 * 1024
         ),

time: 101 us -> 90.6 us (0.90)
  Pallas kernels: 99.8 us -> 89.6 us
    pallas_call x1, Pallas kernels: 91.1 us -> 81 us  [on_device(): pl.pallas_call(functools.partial(kernel, fs, rep), out_shape=out_shape, i...]
where the time goes in v1:
time: 90.6 us; the launch traced here: 90.4 us
  Pallas kernels  89.6 us (99%)
    pallas_call x1, Pallas kernels, on_device(): pl.pallas_call(functools.partial(kernel, fs, rep), out_shape=out_shape, i...  81 us
    pallas_call x1, Pallas kernels, on_device(): pl.pallas_call(functools.partial(apply, float(rank * query_cols * tp), fl...  8.66 us

profile of v1, /device:TPU:0, one launch (start us, length us, event | category | flops | bytes accessed | tf_op | source)
XLA Modules:
  0.0 90.4 jit_solution(18206065398850609673)
XLA Ops:
  0.6 0.0 copy-start.5
  0.6 0.0 copy-start.1
  0.7 0.0 copy-start.4
  0.7 0.0 copy-start
  0.7 0.0 copy-start.3
  0.7 0.0 copy-start.2
  0.7 81.0 %shard_map.152 = (bf16[2,2048,512]{2,1,0:T(8,128)(2,1)S(1)}, bf16[2048,1024]{1,0:T(8,128)(2,1)S(1)}, bf16[2048,256]{1,0:T(8,128)(2,1)S(1)}, bf16[512,1024]{1,0:T...) custom-call(bf16[256,2048]{1,0:T(8,128)(2,1)} %inputs_far.1, ...), custom_call_target="tpu_custom_call" | custom-call | tf_op jit(solution)/shard_map/pallas_call | solution.py:1194
  81.7 0.0 copy-done.5
  81.7 0.0 copy-done.1
  81.7 0.0 copy-done.4
  81.7 0.0 copy-done
  81.7 0.0 copy-done.3
  81.7 0.0 copy-done.2
  81.7 8.7 %shard_map.153 = (f32[512,1024]{1,0:T(8,128)}, f32[512,256]{1,0:T(8,128)}, f32[512,1024]{1,0:T(8,128)}, f32[512,256]{1,0:T(8,128)}, bf16[2048,1024]{1,0:T(8,128)...) custom-call(f32[2,8,128]{2,1,0:T(8,128)S(1)} %get-tuple-element.16.totals, ...), custom_call_target="tpu_custom_call" | custom-call | tf_op jit(solution)/shard_map/pallas_call | solution.py:1235
Async XLA Ops:
  0.6 81.1 %copy-start.5 = (f32[2,128,256]{2,1,0:T(8,128)S(1)}, f32[2,128,256]{2,1,0:T(8,128)}, u32[]{:S(2)}) copy-start(f32[2,128,256]{2,1,0:T(8,128)} %moments_key.1) | copy-start | bytes 786436
  0.6 81.1 %copy-start.1 = (f32[2,128,1024]{2,1,0:T(8,128)S(1)}, f32[2,128,1024]{2,1,0:T(8,128)}, u32[]{:S(2)}) copy-start(f32[2,128,1024]{2,1,0:T(8,128)} %moments_query.1) | copy-start | bytes 3145732
  0.7 81.1 %copy-start.4 = (f32[512,256]{1,0:T(8,128)S(1)}, f32[512,256]{1,0:T(8,128)}, u32[]{:S(2)}) copy-start(f32[512,256]{1,0:T(8,128)} %weight_key.1) | copy-start | bytes 1572868
  0.7 81.1 %copy-start = (f32[512,1024]{1,0:T(8,128)S(1)}, f32[512,1024]{1,0:T(8,128)}, u32[]{:S(2)}) copy-start(f32[512,1024]{1,0:T(8,128)} %weight_query.1) | copy-start | bytes 6291460
  0.7 81.1 %copy-start.3 = (bf16[512,512]{1,0:T(8,128)(2,1)S(1)}, bf16[512,512]{1,0:T(8,128)(2,1)}, u32[]{:S(2)}) copy-start(bf16[512,512]{1,0:T(8,128)(2,1)} %basis_key.3) | copy-start | bytes 1572868
  0.7 81.1 %copy-start.2 = (bf16[512,512]{1,0:T(8,128)(2,1)S(1)}, bf16[512,512]{1,0:T(8,128)(2,1)}, u32[]{:S(2)}) copy-start(bf16[512,512]{1,0:T(8,128)(2,1)} %basis_query.3) | copy-start | bytes 1572868

commit v2 on v1

--- a/solution.py
+++ b/solution.py
@@ -467,14 +467,19 @@
     full_key,
     moments_query_far,
     moments_key_far,
+    step_query,
+    step_key,
+    new_weight_query,
+    new_weight_key,
+    copy_query,
+    copy_key,
+    new_moments_query,
+    new_moments_key,
     basis_all,
     weight_query_all,
     weight_key_all,
     dir_query,
     dir_key,
-    low_query,
-    low_key,
-    totals,
     inputs,
     cot_query,
     cot_key,
@@ -493,30 +498,31 @@
     part_squares,
     squares,
     pair,
-    az_s,
-    az_r,
-    ap_s,
-    ap_r,
-    wz_s,
-    wz_r,
-    wp_s,
-    wp_r,
-    kz_s,
-    kz_r,
-    h1_s,
-    h1_r,
-    h2_s,
-    h2_r,
-    bz_s,
-    bz_r,
-    lp_s,
-    lp_r,
-    dz_s,
-    dz_r,
-    dp_s,
-    dp_r,
-    qz_s,
-    qz_r,
+    line_s,
+    key_s,
+    basis_line_r,
+    query_line_r,
+    key_line_r,
+    hop_s,
+    basis_hop_r,
+    query_hop_r,
+    basis_end_r,
+    query_end_r,
+    halve_s,
+    first_r,
+    second_r,
+    slab_s,
+    slab_r,
+    low_s,
+    low_r,
+    low_end_r,
+    dir_s,
+    dir_r,
+    dir_hop_s,
+    dir_hop_r,
+    dir_end_r,
+    squares_s,
+    squares_r,
     pair_s,
     pair_r,
     local,
@@ -535,7 +541,6 @@
     near = r + 1 - 2 * lax.rem(r, 2)
     far = r + 2 - 4 * (r // 2)
     across = 3 - r
-    pending = []
 
     def when(conds, body):
         if not conds:
@@ -548,10 +553,12 @@
 
     def send(make, *conds):
         when(conds, lambda: make().start())
-        pending.append((make, conds))
-
-    def receive(make, *conds):
-        when(conds, lambda: make().wait_recv())
+
+    def arrived(block, sem, *conds):
+        when(conds, lambda: remote(block, block, sem, sem, tp=1 - c).wait_recv())
+
+    def departed(block, sem, *conds):
+        when(conds, lambda: remote(block, block, sem, sem, tp=1 - c).wait_send())
 
     def sources(d):
         return ((f - d, f >= d), (f + d, f + d < fs))
@@ -605,16 +612,14 @@
 
     def basis_z(source, up, k):
         block = basis_all.at[c, piece(source, r, k)]
-        return remote(
-            block, block, az_s.at[1 - up, source, k], az_r.at[source, k], fs=f + 2 * up - 1
-        )
+        return remote(block, block, line_s.at[0], basis_line_r.at[source, k], fs=f + 2 * up - 1)
 
     def basis_start(x, up, k):
         return remote(
             bases[x].at[rows_of(r * quarter + k * chunk, chunk)],
             basis_all.at[c, piece(f, r, k)],
-            az_s.at[1 - up, f, k],
-            az_r.at[f, k],
+            line_s.at[0],
+            basis_line_r.at[f, k],
             fs=f + 2 * up - 1,
         )
 
@@ -628,9 +633,6 @@
                     pl.when(there)(lambda: basis_start(x, up, k).start())
             pltpu.make_async_copy(bases[x], basis_all.at[c, own_block], local.at[0]).start()
 
-    for k in range(chunks):
-        for up, there in ways:
-            pending.append((functools.partial(basis_z, f, up, k), (there,)))
     for load in loads:
         load.start()
     own_basis = pltpu.make_async_copy(basis_query, basis_all.at[c, own_block], local.at[0])
@@ -640,62 +642,59 @@
 
     targets = (near, far, far, near)
     sent = (r, r, near, far)
-    arriving = (near, far, across, across)
-
-    def basis_hop(k, source, slot, owner):
-        block = basis_all.at[c, piece(source, owner, k), hop_span(slot, rank)]
-        return remote(
-            block, block, ap_s.at[source, slot, k], ap_r.at[source, slot, k], rep=targets[slot]
-        )
-
-    def weight_hop(k, source, slot, owner):
+
+    def basis_hop(k, source, slot):
+        block = basis_all.at[c, piece(source, sent[slot], k), hop_span(slot, rank)]
+        landed = basis_hop_r.at[source, k] if slot < 2 else basis_end_r.at[0]
+        return remote(block, block, hop_s.at[0], landed, rep=targets[slot])
+
+    def weight_hop(k, source, slot):
         width = weight_query_all.shape[1]
-        block = weight_query_all.at[piece(source, owner, k), hop_span(slot, width)]
-        return remote(
-            block, block, wp_s.at[source, slot, k], wp_r.at[source, slot, k], rep=targets[slot]
-        )
+        block = weight_query_all.at[piece(source, sent[slot], k), hop_span(slot, width)]
+        landed = query_hop_r.at[source, k] if slot < 2 else query_end_r.at[source]
+        return remote(block, block, hop_s.at[1], landed, rep=targets[slot])
 
     def spread(hop, source, *there):
         for slot in (0, 1):
-            send(functools.partial(hop, source, slot, sent[slot]), *there)
-
-    def relay(hop, source, *there):
-        for slot in (0, 1):
-            receive(functools.partial(hop, source, slot, arriving[slot]), *there)
-            send(functools.partial(hop, source, slot + 2, sent[slot + 2]), *there)
-
-    def finish(hop, source, *there):
+            send(functools.partial(hop, source, slot), *there)
+
+    def relay(hop, both, sem, source, *there):
+        arrived(both, sem, *there)
         for slot in (2, 3):
-            receive(functools.partial(hop, source, slot, arriving[slot]), *there)
+            send(functools.partial(hop, source, slot), *there)
+
+    def relay_basis(k, source, *there):
+        both = basis_all.at[c, pl.ds(0, 2 * chunk)]
+        relay(functools.partial(basis_hop, k), both, basis_hop_r.at[source, k], source, *there)
+
+    def relay_weight(k, source):
+        both = weight_query_all.at[pl.ds(0, 2 * chunk)]
+        relay(functools.partial(weight_hop, k), both, query_hop_r.at[source, k], source)
 
     def query_z(source, up, k):
         block = weight_query_all.at[piece(source, r, k)]
-        return remote(
-            block, block, wz_s.at[1 - up, source, k], wz_r.at[source, k], fs=f + 2 * up - 1
-        )
+        return remote(block, block, line_s.at[1], query_line_r.at[source, k], fs=f + 2 * up - 1)
 
     def key_z(source, up, k):
-        block = weight_key_all.at[rows_of(source * height + k * (height // chunks), height // chunks)]
-        return remote(
-            block, block, kz_s.at[1 - up, source, k], kz_r.at[source, k], fs=f + 2 * up - 1
-        )
-
-    def launch(line):
-        for k in range(chunks):
+        block = weight_key_all.at[rows_of(source * height, height)]
+        return remote(block, block, key_s.at[up], key_line_r.at[source], fs=f + 2 * up - 1)
+
+    def launch(line, parts=chunks):
+        for k in range(parts):
             for up, there in ways:
                 send(functools.partial(line, f, up, k), there)
 
     def onward(line, d, k):
         below, above = f - d, f + d
-        receive(functools.partial(line, below, 1, k), f >= d)
+        when((f >= d,), lambda: line(below, 1, k).wait_recv())
         if d + 1 < fs:
             send(functools.partial(line, below, 1, k), f >= d, f + 1 < fs)
-        receive(functools.partial(line, above, 0, k), f + d < fs)
+        when((f + d < fs,), lambda: line(above, 0, k).wait_recv())
         if d + 1 < fs:
             send(functools.partial(line, above, 0, k), f + d < fs, f > 0)
 
-    def onward_all(line, d):
-        for k in range(chunks):
+    def onward_all(line, d, parts=chunks):
+        for k in range(parts):
             onward(line, d, k)
 
     for load in loads[:2]:
@@ -710,19 +709,17 @@
             spread(functools.partial(basis_hop, k), source, there)
         if (d, k) == (max(fs - 2, 1), chunks - 1):
             launch(query_z)
-            launch(key_z)
+            launch(key_z, 1)
         if n >= chunks:
             before, j = steps[n - chunks]
             for source, there in sources(before):
-                relay(functools.partial(basis_hop, j), source, there)
+                relay_basis(j, source, there)
     for d, k in steps[-chunks:]:
         for source, there in sources(d):
-            relay(functools.partial(basis_hop, k), source, there)
+            relay_basis(k, source, there)
     onward_all(query_z, 1)
     spread(functools.partial(weight_hop, 0), other(1))
-    for d, k in steps:
-        for source, there in sources(d):
-            finish(functools.partial(basis_hop, k), source, there)
+    arrived(basis_all.at[c, pl.ds(0, (fs - 1) * quarter)], basis_end_r.at[0])
     own_basis.wait()
     for load in loads[2:]:
         load.wait()
@@ -769,8 +766,8 @@
         return remote(
             part.at[columns_of(g), owner, pl.ds(h * half, half)],
             got_first.at[h, w, columns_of(g)],
-            h1_s.at[h, w, g],
-            h1_r.at[h, w, g],
+            halve_s.at[0],
+            (first_r, second_r)[w].at[g],
             rep=mates[h][0],
         )
 
@@ -778,46 +775,44 @@
         return remote(
             pair_sum.at[h, columns_of(g)],
             got_second.at[h, columns_of(g)],
-            h2_s.at[h, g],
-            h2_r.at[h, g],
+            halve_s.at[1],
+            second_r.at[g],
             rep=mates[h][1],
         )
 
     def start_first(g, w):
         for h in range(2):
-            send(functools.partial(first_hop, h, g, w))
+            first_hop(h, g, w).start()
 
     def start_second(g):
+        arrived(got_first.at[:, 0, columns_of(g)], first_r.at[g])
         for h in range(2):
-            receive(functools.partial(first_hop, h, g, 0))
             for u in range(streams[g][0], sum(streams[g])):
                 pair_sum[h, u] = (
                     part[u, mates[h][1], spans[h]].astype(f32) + got_first[h, 0, u].astype(f32)
                 ).astype(bf16)
-            send(functools.partial(second_hop, h, g))
+            second_hop(h, g).start()
 
     def slab_z(g, source, target):
         return remote(
             slab.at[columns_of(g), rows_of(target * own, own)],
             slab_recv.at[source, columns_of(g)],
-            bz_s.at[g, target],
-            bz_r.at[g, source],
+            slab_s.at[0],
+            slab_r.at[g],
             fs=target,
         )
 
     def end_rep(g):
+        arrived(got_first.at[:, :, columns_of(g)], second_r.at[g])
         for h in range(2):
-            receive(functools.partial(first_hop, h, g, 1))
-            receive(functools.partial(second_hop, h, g))
             for u in range(streams[g][0], sum(streams[g])):
                 slab[u, spans[h]] = (
                     part[u, r, spans[h]].astype(f32)
                     + got_first[h, 1, u].astype(f32)
                     + got_second[h, u].astype(f32)
                 ).astype(bf16)
-        for d in range(fs - 1, 0, -1):
-            for target, there in sources(d):
-                send(functools.partial(slab_z, g, f, target), there)
+        for n in range(fs - 1, 0, -1):
+            slab_z(g, f, other(n)).start()
         for u in range(streams[g][0], sum(streams[g])):
             slab_recv[f, u] = slab[u, rows_of(f * own, own)]
 
@@ -835,7 +830,7 @@
     for k in range(chunks):
         spread(functools.partial(weight_hop, k), other(2))
 
-    directions, lows = (dir_query, dir_key), (low_query, low_key)
+    directions, new_moments = (dir_query, dir_key), (new_moments_query, new_moments_key)
     moments = (moments_query, moments_key)
 
     def place(u):
@@ -862,82 +857,71 @@
         for u in range(streams[g][0], sum(streams[g])):
             x, span = place(u)
             low = low_all[owner, u].astype(f32)
-            lows[x][mine, span] = low
             first = 0.9 * moments[x][0, mine, span] + 0.1 * low
             second = 0.95 * moments[x][1, mine, span] + 0.05 * low * low
+            new_moments[x][0, mine, span] = first
+            new_moments[x][1, mine, span] = second
             normed = first / (jnp.sqrt(second) + 1e-08)
             directions[x][dir_rows(f, owner), span] = normed.astype(bf16)
             sums[x] = sums[x] + jnp.sum((normed * normed).reshape(own // 8, 8, LANES), axis=0)
         for x in range(2):
             part_squares[owner, g, x] = sums[x]
 
-    def low_hop(g, slot, owner):
-        block = low_all.at[owner, columns_of(g)]
-        return remote(block, block, lp_s.at[slot, g], lp_r.at[slot, g], rep=targets[slot])
-
-    def dir_z(g, n, source, target):
-        x, start, size = pieces(g)[n]
-        block = directions[x].at[dir_rows(source, r), pl.ds(start, size)]
-        return remote(block, block, dz_s.at[g, n, target], dz_r.at[g, n, source], fs=target)
-
-    def dir_hop(g, n, slot, source, owner):
-        x, start, size = pieces(g)[n]
-        block = directions[x].at[dir_rows(source, owner), pl.ds(start, size)]
-        return remote(
-            block,
-            block,
-            dp_s.at[g, n, slot, source],
-            dp_r.at[g, n, slot, source],
-            rep=targets[slot],
-        )
+    def low_hop(g, slot):
+        block = low_all.at[sent[slot], columns_of(g)]
+        landed = low_r.at[g] if slot == g else low_end_r.at[0]
+        return remote(block, block, low_s.at[0], landed, rep=targets[slot])
+
+    def dir_blocks(g, source, owner):
+        return [
+            directions[x].at[dir_rows(source, owner), pl.ds(start, size)]
+            for x, start, size in pieces(g)
+        ]
+
+    def dir_z(g, target):
+        for block in dir_blocks(g, f, r):
+            remote(block, block, dir_s.at[0], dir_r.at[g, f], fs=target).start()
+
+    def dir_hop(g, slot, n):
+        landed = dir_hop_r.at[n, g] if slot == g else dir_end_r.at[n]
+        for block in dir_blocks(g, other(n), sent[slot]):
+            remote(block, block, dir_hop_s.at[n], landed, rep=targets[slot]).start()
 
     def end_fs(g):
-        for d in range(1, fs):
-            for source, there in sources(d):
-                receive(functools.partial(slab_z, g, source, source), there)
+        arrived(slab_recv.at[pl.ds(0, fs - 1), columns_of(g)], slab_r.at[g])
         for u in range(streams[g][0], sum(streams[g])):
             value = slab_recv[0, u].astype(f32)
             for q in range(1, fs):
                 value = value + slab_recv[q, u].astype(f32)
             low_all[r, u] = value.astype(bf16)
         for slot in (0, 1):
-            send(functools.partial(low_hop, g, slot, r))
+            low_hop(g, slot).start()
         update(g, r)
-        for d in range(fs - 1, 0, -1):
-            for target, there in sources(d):
-                for n in range(len(pieces(g))):
-                    send(functools.partial(dir_z, g, n, f, target), there)
+        for n in range(fs - 1, 0, -1):
+            dir_z(g, other(n))
 
     end_fs(0)
     end_fs(1)
 
-    def spread_dir(g, d):
-        for source, there in sources(d):
-            for n in range(len(pieces(g))):
-                receive(functools.partial(dir_z, g, n, source, source), there)
-                for slot in (0, 1):
-                    send(functools.partial(dir_hop, g, n, slot, source, r), there)
-
-    def relay_dir(d):
-        for source, there in sources(d):
-            for g in range(2):
-                for n in range(len(pieces(g))):
-                    receive(functools.partial(dir_hop, g, n, g, source, arriving[g]), there)
-                    send(functools.partial(dir_hop, g, n, g + 2, source, sent[g + 2]), there)
-
-    def finish_dir(d):
-        for source, there in sources(d):
-            for g in range(2):
-                for n in range(len(pieces(g))):
-                    receive(functools.partial(dir_hop, g, n, 1 - g, source, arriving[1 - g]), there)
-                    receive(functools.partial(dir_hop, g, n, g + 2, source, across), there)
-
-    onward_all(key_z, 1)
+    def spread_dir(g, n):
+        arrived(low_all.at[r, columns_of(g)], dir_r.at[g, other(n)])
+        for slot in (0, 1):
+            dir_hop(g, slot, n)
+
+    def relay_dir(n):
+        for g in range(2):
+            arrived(low_all.at[r, columns_of(g)], dir_hop_r.at[n, g])
+            dir_hop(g, g + 2, n)
+
+    def finish_dir(n):
+        arrived(low_all.at[pl.ds(0, 2)], dir_end_r.at[n])
+
+    onward_all(key_z, 1, 1)
     for k in range(chunks):
-        relay(functools.partial(weight_hop, k), other(1))
+        relay_weight(k, other(1))
     for g in range(2):
-        receive(functools.partial(low_hop, g, g, arriving[g]))
-        send(functools.partial(low_hop, g, g + 2, sent[g + 2]))
+        arrived(low_all.at[r, columns_of(g)], low_r.at[g])
+        low_hop(g, g + 2).start()
     spread_dir(0, 1)
     spread_dir(1, 1)
     for d in range(2, fs):
@@ -946,16 +930,15 @@
         relay_dir(d - 1)
     relay_dir(fs - 1)
     for k in range(chunks):
-        relay(functools.partial(weight_hop, k), other(2))
+        relay_weight(k, other(2))
     for n in range(3, fs):
         for k in range(chunks):
             onward(query_z, n, k)
             spread(functools.partial(weight_hop, k), other(n))
     for d in range(2, fs - 1):
-        onward_all(key_z, d)
+        onward_all(key_z, d, 1)
+    arrived(low_all.at[pl.ds(0, 2)], low_end_r.at[0])
     for g in range(2):
-        receive(functools.partial(low_hop, g, 1 - g, arriving[1 - g]))
-        receive(functools.partial(low_hop, g, g + 2, across))
         for j in range(1, rep):
             update(g, beside(j))
     for x in range(2):
@@ -964,16 +947,10 @@
             total = total + (part_squares[q, 0, x] + part_squares[q, 1, x])
         squares[f, x] = total
 
-    def squares_z(source, target):
-        block = squares.at[source]
-        return remote(block, block, qz_s.at[target], qz_r.at[source], fs=target)
-
-    for d in range(1, fs):
-        for target, there in sources(d):
-            send(functools.partial(squares_z, f, target), there)
-    for d in range(1, fs):
-        for source, there in sources(d):
-            receive(functools.partial(squares_z, source, source), there)
+    mine = squares.at[f]
+    for n in range(1, fs):
+        remote(mine, mine, squares_s.at[0], squares_r.at[0], fs=other(n)).start()
+    arrived(squares.at[pl.ds(0, fs - 1)], squares_r.at[0])
     total = squares[0]
     for q in range(1, fs):
         total = total + squares[q]
@@ -983,20 +960,100 @@
 
     for d in range(1, fs):
         finish_dir(d)
+    total_back.wait_recv()
+    totals = pair[0] + pair[1]
+    weights_all, copies = (weight_query_all, weight_key_all), (copy_query, copy_key)
+    scales = [
+        lax.rsqrt(jnp.sum(totals[x], keepdims=True) / (pair.shape[0] * rank * copies[x].shape[1]) + 1e-06)
+        for x in range(2)
+    ]
+
+    def product(x, span, columns):
+        return scales[x] * jnp.dot(
+            basis_all[x, span], directions[x][:, columns], preferred_element_type=f32
+        )
+
+    def column_blocks(x):
+        wide = copies[x].shape[1]
+        width = 2 * LANES if wide % (2 * LANES) == 0 else LANES
+        return [slice(n, n + width) for n in range(0, wide, width)]
+
+    def copy_rows(x, start, size):
+        span = rows_of(start, size)
+        for columns in column_blocks(x):
+            weight = weights_all[x][span, columns].astype(f32)
+            copies[x][span, columns] = (weight - 0.02 * product(x, span, columns)).astype(bf16)
+
+    swap_back.wait_recv()
+    for x, weight, step_out, new_out in (
+        (0, loaded_query, step_query, new_weight_query),
+        (1, loaded_key, step_key, new_weight_key),
+    ):
+        for columns in column_blocks(x):
+            step = product(x, own_block, columns)
+            step_out[:, columns] = step
+            new = weight[:, columns] - 0.02 * step
+            new_out[:, columns] = new
+            copies[x][own_block, columns] = new.astype(bf16)
+
+    def relay_last(k):
+        for n in range(3, fs):
+            relay_weight(k, other(n))
+
+    def finish_weight(n):
+        arrived(weight_query_all.at[pl.ds(0, quarter)], query_end_r.at[other(n)])
+
+    finish_weight(1)
+    copy_rows(0, other(1) * height, height)
+    relay_last(0)
+    finish_weight(2)
+    copy_rows(0, other(2) * height, height)
+    relay_last(1)
+    for n in (1, 2):
+        copy_rows(1, other(n) * height, height)
     for n in range(3, fs):
-        for k in range(chunks):
-            relay(functools.partial(weight_hop, k), other(n))
-    onward_all(key_z, fs - 1)
+        for owner in (r, near, far):
+            copy_rows(0, other(n) * height + owner * quarter, quarter)
+    for d in range(max(fs - 1, 3), fs):
+        onward_all(key_z, d, 1)
+    for n in range(3, fs):
+        copy_rows(1, other(n) * height, height)
+    for n in range(3, fs):
+        finish_weight(n)
+        copy_rows(0, other(n) * height + across * quarter, quarter)
+    edge = (f == 0) | (f == fs - 1)
+    hops = (fs - 1) * (rep - 1) * quarter
+    for n, block in ((0, basis_all.at[c]), (1, weight_query_all)):
+        departed(block.at[pl.ds(0, quarter)], line_s.at[n], edge)
+        departed(block.at[pl.ds(0, (fs + 1) * quarter)], line_s.at[n], jnp.logical_not(edge))
+        departed(block.at[pl.ds(0, hops)], hop_s.at[n])
+    for n in range(fs):
+        if n < fs - 1:
+            departed(weight_key_all.at[pl.ds(0, (n + 1) * height)], key_s.at[1], f == n)
+        if n > 0:
+            departed(weight_key_all.at[pl.ds(0, (fs - n) * height)], key_s.at[0], f == n)
+    departed(got_first, halve_s.at[0])
+    departed(pair_sum, halve_s.at[1])
+    departed(slab_recv.at[pl.ds(0, fs - 1)], slab_s.at[0])
+    departed(low_all.at[pl.ds(0, rep - 1)], low_s.at[0])
+    departed(slab_recv.at[pl.ds(0, fs - 1)], dir_s.at[0])
     for n in range(1, fs):
-        for k in range(chunks):
-            finish(functools.partial(weight_hop, k), other(n))
-    total_back.wait_recv()
-    totals[...] = pair[0] + pair[1]
-    for make, conds in pending:
-        when(conds, lambda: make().wait_send())
-    swap_back.wait_recv()
+        departed(low_all.at[pl.ds(0, rep - 1)], dir_hop_s.at[n])
+    departed(squares.at[pl.ds(0, fs - 1)], squares_s.at[0])
     for copy in (factor_copy, swap, total_copy):
         copy.wait_send()
+
+
+def write_out(*refs):
+    count = len(refs) // 2
+    copies = [
+        pltpu.make_async_copy(source, target, refs[-1].at[n])
+        for n, (source, target) in enumerate(zip(refs[:count], refs[count : 2 * count]))
+    ]
+    for copy in copies:
+        copy.start()
+    for copy in copies:
+        copy.wait()
 
 
 def apply(
@@ -1079,69 +1136,127 @@
     bf16, f32 = jnp.bfloat16, jnp.float32
     dma = pltpu.SemaphoreType.DMA
     shape = jax.ShapeDtypeStruct
-    out_shape = (
-        shape((2, height * fs, rank), bf16),
+    owned = tuple(
+        shape((height, columns), f32) for columns in (query_cols, key_cols, query_cols, key_cols)
+    )
+    results = owned + (
         shape((height * fs, query_cols), bf16),
         shape((height * fs, key_cols), bf16),
-        shape((rank, query_cols), bf16),
-        shape((rank, key_cols), bf16),
-        shape((rows, query_cols), f32),
-        shape((rows, key_cols), f32),
-        shape((2, 8, LANES), f32),
+        shape((2, rows, query_cols), f32),
+        shape((2, rows, key_cols), f32),
     )
     own, units = rows // rep, (query_cols + key_cols) // LANES
-    if own % 16 == 0 and fs % 2 == 0 and units % 2 == 0 and rows % rep == 0:
-        kernel, out_specs = exchange_grid, (vmem,) * 8
-        scratch = [
-            pltpu.VMEM((tokens, inputs.shape[1]), bf16),
-            pltpu.VMEM((tokens, query_cols), bf16),
-            pltpu.VMEM((tokens, key_cols), bf16),
-            pltpu.VMEM((2, rows, query_cols), f32),
-            pltpu.VMEM((2, rows, key_cols), f32),
-            pltpu.VMEM((height, query_cols), f32),
-            pltpu.VMEM((height, key_cols), f32),
-            pltpu.VMEM((2, rank, tokens), bf16),
-            pltpu.VMEM((units, rep, rows, LANES), bf16),
-            pltpu.VMEM((2, 2, units, rows // 2, LANES), bf16),
-            pltpu.VMEM((2, units, rows // 2, LANES), bf16),
-            pltpu.VMEM((2, units, rows // 2, LANES), bf16),
-            pltpu.VMEM((units, rows, LANES), bf16),
-            pltpu.VMEM((fs, units, own, LANES), bf16),
-            pltpu.VMEM((rep, units, own, LANES), bf16),
-            pltpu.VMEM((rep, 2, 2, 8, LANES), f32),
-            pltpu.VMEM((fs, 2, 8, LANES), f32),
-            pltpu.VMEM((2, 2, 8, LANES), f32),
-            dma((2, fs, 2)),
-            dma((fs, 2)),
-            dma((fs, rep, 2)),
-            dma((fs, rep, 2)),
-            dma((2, fs, 2)),
-            dma((fs, 2)),
-            dma((fs, rep, 2)),
-            dma((fs, rep, 2)),
-            dma((2, fs, 2)),
-            dma((fs, 2)),
-            dma((2, 2, 2)),
-            dma((2, 2, 2)),
-            dma((2, 2)),
-            dma((2, 2)),
-            dma((2, fs)),
-            dma((2, fs)),
-            dma((4, 2)),
-            dma((4, 2)),
-            dma((2, 2, fs)),
-            dma((2, 2, fs)),
-            dma((2, 2, 4, fs)),
-            dma((2, 2, 4, fs)),
-            dma((fs,)),
-            dma((fs,)),
-            dma((3,)),
-            dma((3,)),
-            dma((8,)),
-        ]
-    else:
-        kernel, out_specs = exchange, (vmem, hbm, hbm, vmem, vmem, vmem, vmem, vmem)
-        scratch = [
+    if own % 16 == 0 and fs % 2 == 0 and fs > 2 and units % 2 == 0:
+        fresh = pl.pallas_call(
+            functools.partial(exchange_grid, fs, rep),
+            out_shape=results,
+            in_specs=[pl.BlockSpec(memory_space=pltpu.HBM)] * 9,
+            out_specs=(vmem,) * 8,
+            scratch_shapes=[
+                pltpu.VMEM((2, height * fs, rank), bf16),
+                pltpu.VMEM((height * fs, query_cols), bf16),
+                pltpu.VMEM((height * fs, key_cols), bf16),
+                pltpu.VMEM((rank, query_cols), bf16),
+                pltpu.VMEM((rank, key_cols), bf16),
+                pltpu.VMEM((tokens, inputs.shape[1]), bf16),
+                pltpu.VMEM((tokens, query_cols), bf16),
+                pltpu.VMEM((tokens, key_cols), bf16),
+                pltpu.VMEM((2, rows, query_cols), f32),
+                pltpu.VMEM((2, rows, key_cols), f32),
+                pltpu.VMEM((height, query_cols), f32),
+                pltpu.VMEM((height, key_cols), f32),
+                pltpu.VMEM((2, rank, tokens), bf16),
+                pltpu.VMEM((units, rep, rows, LANES), bf16),
+                pltpu.VMEM((2, 2, units, rows // 2, LANES), bf16),
+                pltpu.VMEM((2, units, rows // 2, LANES), bf16),
+                pltpu.VMEM((2, units, rows // 2, LANES), bf16),
+                pltpu.VMEM((units, rows, LANES), bf16),
+                pltpu.VMEM((fs, units, own, LANES), bf16),
+                pltpu.VMEM((rep, units, own, LANES), bf16),
+                pltpu.VMEM((rep, 2, 2, 8, LANES), f32),
+                pltpu.VMEM((fs, 2, 8, LANES), f32),
+                pltpu.VMEM((2, 2, 8, LANES), f32),
+                dma((2,)),
+                dma((2,)),
+                dma((fs, 2)),
+                dma((fs, 2)),
+                dma((fs,)),
+                dma((2,)),
+                dma((fs, 2)),
+                dma((fs, 2)),
+                dma((1,)),
+                dma((fs,)),
+                dma((2,)),
+                dma((2,)),
+                dma((2,)),
+                dma((1,)),
+                dma((2,)),
+                dma((1,)),
+                dma((2,)),
+                dma((1,)),
+                dma((1,)),
+                dma((2, fs)),
+                dma((fs,)),
+                dma((fs, 2)),
+                dma((fs,)),
+                dma((1,)),
+                dma((1,)),
+                dma((3,)),
+                dma((3,)),
+                dma((8,)),
+            ],
+            compiler_params=pltpu.CompilerParams(
+                collective_id=0, has_side_effects=True, vmem_limit_bytes=40 * 1024 * 1024
+            ),
+        )(
+            *(
+                pltpu.with_memory_space_constraint(operand, pltpu.HBM)
+                for operand in (
+                    inputs,
+                    cot_query,
+                    cot_key,
+                    basis_query,
+                    basis_key,
+                    weight_query,
+                    weight_key,
+                    moments_query,
+                    moments_key,
+                )
+            )
+        )
+        return pl.pallas_call(
+            write_out,
+            out_shape=results,
+            in_specs=[vmem] * 8,
+            out_specs=(hbm,) * 8,
+            scratch_shapes=[dma((8,))],
+            compiler_params=pltpu.CompilerParams(vmem_limit_bytes=32 * 1024 * 1024),
+        )(*fresh)
+
+    (
+        basis_all,
+        weight_query_all,
+        weight_key_all,
+        dir_query,
+        dir_key,
+        low_query,
+        low_key,
+        totals,
+    ) = pl.pallas_call(
+        functools.partial(exchange, fs, rep),
+        out_shape=(
+            shape((2, height * fs, rank), bf16),
+            shape((height * fs, query_cols), bf16),
+            shape((height * fs, key_cols), bf16),
+            shape((rank, query_cols), bf16),
+            shape((rank, key_cols), bf16),
+            shape((rows, query_cols), f32),
+            shape((rows, key_cols), f32),
+            shape((2, 8, LANES), f32),
+        ),
+        in_specs=[pl.BlockSpec(memory_space=pltpu.HBM)] * 9,
+        out_specs=(vmem, hbm, hbm, vmem, vmem, vmem, vmem, vmem),
+        scratch_shapes=[
             pltpu.VMEM((tokens, inputs.shape[1]), bf16),
             pltpu.VMEM((tokens, query_cols), bf16),
             pltpu.VMEM((tokens, key_cols), bf16),
@@ -1181,22 +1296,7 @@
             dma((3,)),
             dma((3,)),
             dma((10,)),
-        ]
-    (
-        basis_all,
-        weight_query_all,
-        weight_key_all,
-        dir_query,
-        dir_key,
-        low_query,
-        low_key,
-        totals,
-    ) = pl.pallas_call(
-        functools.partial(kernel, fs, rep),
-        out_shape=out_shape,
-        in_specs=[pl.BlockSpec(memory_space=pltpu.HBM)] * 9,
-        out_specs=out_specs,
-        scratch_shapes=scratch,
+        ],
         compiler_params=pltpu.CompilerParams(
             collective_id=0, has_side_effects=True, vmem_limit_bytes=32 * 1024 * 1024
         ),
@@ -1226,9 +1326,6 @@
     def banded(*dims):
         return pl.BlockSpec(dims, lambda i: (i, 0))
 
-    owned = tuple(
-        shape((height, columns), f32) for columns in (query_cols, key_cols, query_cols, key_cols)
-    )
     owned_specs = tuple(
         banded(short, columns) for columns in (query_cols, key_cols, query_cols, key_cols)
     )
@@ -1237,13 +1334,7 @@
             apply, float(rank * query_cols * tp), float(rank * key_cols * tp)
         ),
         grid=(steps,),
-        out_shape=owned
-        + (
-            shape((height * fs, query_cols), bf16),
-            shape((height * fs, key_cols), bf16),
-            shape((2, rows, query_cols), f32),
-            shape((2, rows, key_cols), f32),
-        ),
+        out_shape=results,
         in_specs=[
             fixed(2, 8, LANES),
             fixed(rank, query_cols),

time: 90.6 us -> 83.7 us (0.924)
  Pallas kernels: 89.6 us -> 82.9 us
    pallas_call x2, Pallas kernels: 89.6 us -> 82.9 us  [the longest x1 78.5 us: on_device(): pl.pallas_call(functools.partial(exchange_grid, fs, rep), out_shape=resul...]
where the time goes in v2:
time: 83.7 us; the launch traced here: 83.6 us
  Pallas kernels  82.9 us (99%)
    pallas_call x1, Pallas kernels, on_device(): pl.pallas_call(functools.partial(exchange_grid, fs, rep), out_shape=resul...  78.5 us
    pallas_call x1, Pallas kernels, on_device(): pl.pallas_call(write_out, out_shape=results, in_specs=[vmem] * 8, out_spe...  4.38 us

profile of v2, /device:TPU:0, one launch (start us, length us, event | category | flops | bytes accessed | tf_op | source)
XLA Modules:
  0.0 83.6 jit_solution(6727846953083994059)
XLA Ops:
  0.6 78.5 %shard_map.152 = (f32[512,1024]{1,0:T(8,128)S(1)}, f32[512,256]{1,0:T(8,128)S(1)}, f32[512,1024]{1,0:T(8,128)S(1)}, f32[512,256]{1,0:T(8,128)S(1)}, bf16[2048,10...) custom-call(bf16[256,2048]{1,0:T(8,128)(2,1)} %inputs_far.1, ...), custom_call_target="tpu_custom_call" | custom-call | tf_op jit(solution)/shard_map/pallas_call | solution.py:1150
  79.2 4.4 %shard_map.153 = (f32[512,1024]{1,0:T(8,128)}, f32[512,256]{1,0:T(8,128)}, f32[512,1024]{1,0:T(8,128)}, f32[512,256]{1,0:T(8,128)}, bf16[2048,1024]{1,0:T(8,128)...) custom-call(f32[512,1024]{1,0:T(8,128)S(1)} %get-tuple-element.16.refs_0_, ...), custom_call_target="tpu_custom_call" | custom-call | tf_op jit(solution)/shard_map/pallas_call | solution.py:1227

commit v3 on v2

--- a/solution.py
+++ b/solution.py
@@ -571,9 +571,11 @@
 
     chunks = 2
     chunk = quarter // chunks
-
-    def piece(source, owner, k):
-        return rows_of(source * height + owner * quarter + k * chunk, chunk)
+    fine = basis_line_r.shape[1]
+
+    def piece(source, owner, k, parts=chunks):
+        size = quarter // parts
+        return rows_of(source * height + owner * quarter + k * size, size)
 
     mirror = f // (fs // 2)
     place_in_half = f + mirror * (fs - 1 - 2 * f)
@@ -598,6 +600,16 @@
             )
         )
     ]
+    bases = (basis_query, basis_key)
+    for x in range(2):
+
+        @pl.when(c == x)
+        def load_basis():
+            pltpu.make_async_copy(bases[x], basis_all.at[c, own_block], local.at[0]).start()
+
+    for load in loads:
+        load.start()
+    own_basis = pltpu.make_async_copy(basis_query, basis_all.at[c, own_block], local.at[0])
     barrier = pltpu.get_barrier_semaphore()
     for i in range(1, fs):
         pl.semaphore_signal(
@@ -608,35 +620,13 @@
     pl.semaphore_signal(barrier, inc=1, device_id={"tp": 1 - c}, device_id_type=MESH)
     pl.semaphore_wait(barrier, fs + 2)
 
-    bases = (basis_query, basis_key)
-
     def basis_z(source, up, k):
-        block = basis_all.at[c, piece(source, r, k)]
+        block = basis_all.at[c, piece(source, r, k, fine)]
         return remote(block, block, line_s.at[0], basis_line_r.at[source, k], fs=f + 2 * up - 1)
 
-    def basis_start(x, up, k):
-        return remote(
-            bases[x].at[rows_of(r * quarter + k * chunk, chunk)],
-            basis_all.at[c, piece(f, r, k)],
-            line_s.at[0],
-            basis_line_r.at[f, k],
-            fs=f + 2 * up - 1,
-        )
-
     ways = ((1, f + 1 < fs), (0, f > 0))
-    for x in range(2):
-
-        @pl.when(c == x)
-        def start_basis():
-            for k in range(chunks):
-                for up, there in ways:
-                    pl.when(there)(lambda: basis_start(x, up, k).start())
-            pltpu.make_async_copy(bases[x], basis_all.at[c, own_block], local.at[0]).start()
-
-    for load in loads:
-        load.start()
-    own_basis = pltpu.make_async_copy(basis_query, basis_all.at[c, own_block], local.at[0])
-
+    edge = (f == 0) | (f == fs - 1)
+    inner = (f > 0) & (f < fs - 1)
     def hop_span(slot, width):
         return (pl.ds(0, width), pl.ds(0, width), pl.ds(0, width // 2), pl.ds(width // 2, width // 2))[slot]
 
@@ -644,7 +634,7 @@
     sent = (r, r, near, far)
 
     def basis_hop(k, source, slot):
-        block = basis_all.at[c, piece(source, sent[slot], k), hop_span(slot, rank)]
+        block = basis_all.at[c, piece(source, sent[slot], k, fine), hop_span(slot, rank)]
         landed = basis_hop_r.at[source, k] if slot < 2 else basis_end_r.at[0]
         return remote(block, block, hop_s.at[0], landed, rep=targets[slot])
 
@@ -664,7 +654,7 @@
             send(functools.partial(hop, source, slot), *there)
 
     def relay_basis(k, source, *there):
-        both = basis_all.at[c, pl.ds(0, 2 * chunk)]
+        both = basis_all.at[c, pl.ds(0, 2 * (quarter // fine))]
         relay(functools.partial(basis_hop, k), both, basis_hop_r.at[source, k], source, *there)
 
     def relay_weight(k, source):
@@ -684,43 +674,44 @@
             for up, there in ways:
                 send(functools.partial(line, f, up, k), there)
 
-    def onward(line, d, k):
-        below, above = f - d, f + d
-        when((f >= d,), lambda: line(below, 1, k).wait_recv())
-        if d + 1 < fs:
-            send(functools.partial(line, below, 1, k), f >= d, f + 1 < fs)
-        when((f + d < fs,), lambda: line(above, 0, k).wait_recv())
-        if d + 1 < fs:
-            send(functools.partial(line, above, 0, k), f + d < fs, f > 0)
+    def onward(line, d, k, *conds):
+        for source, there, up, more in (
+            (f - d, f >= d, 1, f + 1 < fs),
+            (f + d, f + d < fs, 0, f > 0),
+        ):
+            when((there, *conds), lambda: line(source, up, k).wait_recv())
+            if d + 1 < fs:
+                send(functools.partial(line, source, up, k), there, more, *conds)
 
     def onward_all(line, d, parts=chunks):
         for k in range(parts):
             onward(line, d, k)
 
+    own_basis.wait()
+    launch(basis_z, fine)
     for load in loads[:2]:
         load.wait()
     weight_query_all[own_block, :] = loaded_query[...].astype(bf16)
     weight_key_all[own_block, :] = loaded_key[...].astype(bf16)
 
-    steps = [(d, k) for d in range(1, fs) for k in range(chunks)]
+    steps = [(d, k) for d in range(1, fs) for k in range(fine)]
     for n, (d, k) in enumerate(steps):
         onward(basis_z, d, k)
         for source, there in sources(d):
             spread(functools.partial(basis_hop, k), source, there)
-        if (d, k) == (max(fs - 2, 1), chunks - 1):
+        if (d, k) == (max(fs - 2, 1), fine - 1):
             launch(query_z)
-            launch(key_z, 1)
-        if n >= chunks:
-            before, j = steps[n - chunks]
+        if n >= 6:
+            before, j = steps[n - 6]
             for source, there in sources(before):
                 relay_basis(j, source, there)
-    for d, k in steps[-chunks:]:
+    for d, k in steps[-6:]:
         for source, there in sources(d):
             relay_basis(k, source, there)
     onward_all(query_z, 1)
+    launch(key_z, 1)
     spread(functools.partial(weight_hop, 0), other(1))
     arrived(basis_all.at[c, pl.ds(0, (fs - 1) * quarter)], basis_end_r.at[0])
-    own_basis.wait()
     for load in loads[2:]:
         load.wait()
 
@@ -826,8 +817,8 @@
         spread(functools.partial(weight_hop, k), other(1))
     end_rep(0)
     end_rep(1)
-    onward_all(query_z, 2)
     for k in range(chunks):
+        when((edge,), lambda: query_z(other(2), 1, k).wait_recv())
         spread(functools.partial(weight_hop, k), other(2))
 
     directions, new_moments = (dir_query, dir_key), (new_moments_query, new_moments_key)
@@ -874,17 +865,17 @@
 
     def dir_blocks(g, source, owner):
         return [
-            directions[x].at[dir_rows(source, owner), pl.ds(start, size)]
+            (x, directions[x].at[dir_rows(source, owner), pl.ds(start, size)])
             for x, start, size in pieces(g)
         ]
 
-    def dir_z(g, target):
-        for block in dir_blocks(g, f, r):
-            remote(block, block, dir_s.at[0], dir_r.at[g, f], fs=target).start()
+    def dir_line(g, source, up):
+        for x, block in dir_blocks(g, source, r):
+            remote(block, block, dir_s.at[x], dir_r.at[g, source], fs=f + 2 * up - 1).start()
 
     def dir_hop(g, slot, n):
         landed = dir_hop_r.at[n, g] if slot == g else dir_end_r.at[n]
-        for block in dir_blocks(g, other(n), sent[slot]):
+        for x, block in dir_blocks(g, other(n), sent[slot]):
             remote(block, block, dir_hop_s.at[n], landed, rep=targets[slot]).start()
 
     def end_fs(g):
@@ -897,16 +888,26 @@
         for slot in (0, 1):
             low_hop(g, slot).start()
         update(g, r)
-        for n in range(fs - 1, 0, -1):
-            dir_z(g, other(n))
+        for up, there in ways:
+            when((there,), lambda: dir_line(g, f, up))
 
     end_fs(0)
     end_fs(1)
 
-    def spread_dir(g, n):
-        arrived(low_all.at[r, columns_of(g)], dir_r.at[g, other(n)])
-        for slot in (0, 1):
-            dir_hop(g, slot, n)
+    def onward_dir(d):
+        for g in range(2):
+            for source, there, up, more in (
+                (f - d, f >= d, 1, f + 1 < fs),
+                (f + d, f + d < fs, 0, f > 0),
+            ):
+                arrived(low_all.at[r, columns_of(g)], dir_r.at[g, source], there)
+                if d + 1 < fs:
+                    when((there, more), lambda: dir_line(g, source, up))
+
+    def spread_dir(n, *conds):
+        for g in range(2):
+            for slot in (0, 1):
+                when(conds, lambda: dir_hop(g, slot, n))
 
     def relay_dir(n):
         for g in range(2):
@@ -916,27 +917,22 @@
     def finish_dir(n):
         arrived(low_all.at[pl.ds(0, 2)], dir_end_r.at[n])
 
-    onward_all(key_z, 1, 1)
     for k in range(chunks):
         relay_weight(k, other(1))
+    onward_dir(1)
+    spread_dir(1)
+    spread_dir(2, inner)
     for g in range(2):
         arrived(low_all.at[r, columns_of(g)], low_r.at[g])
         low_hop(g, g + 2).start()
-    spread_dir(0, 1)
-    spread_dir(1, 1)
-    for d in range(2, fs):
-        spread_dir(0, d)
-        spread_dir(1, d)
-        relay_dir(d - 1)
-    relay_dir(fs - 1)
+    onward_dir(2)
+    spread_dir(2, edge)
+    spread_dir(3, inner)
     for k in range(chunks):
-        relay_weight(k, other(2))
-    for n in range(3, fs):
-        for k in range(chunks):
-            onward(query_z, n, k)
-            spread(functools.partial(weight_hop, k), other(n))
-    for d in range(2, fs - 1):
-        onward_all(key_z, d, 1)
+        onward(query_z, 2, k, inner)
+    relay_dir(1)
+    onward_dir(3)
+    spread_dir(3, edge)
     arrived(low_all.at[pl.ds(0, 2)], low_end_r.at[0])
     for g in range(2):
         for j in range(1, rep):
@@ -950,6 +946,22 @@
     mine = squares.at[f]
     for n in range(1, fs):
         remote(mine, mine, squares_s.at[0], squares_r.at[0], fs=other(n)).start()
+    onward_all(key_z, 1, 1)
+    relay_dir(2)
+    relay_dir(3)
+    for n in range(3, fs):
+        for k in range(chunks):
+            onward(query_z, n, k)
+            spread(functools.partial(weight_hop, k), other(n))
+    for k in range(chunks):
+        relay_weight(k, other(2))
+    def relay_last(k):
+        for n in range(3, fs):
+            relay_weight(k, other(n))
+
+    def finish_weight(n):
+        arrived(weight_query_all.at[pl.ds(0, quarter)], query_end_r.at[other(n)])
+
     arrived(squares.at[pl.ds(0, fs - 1)], squares_r.at[0])
     total = squares[0]
     for q in range(1, fs):
@@ -957,7 +969,6 @@
     pair[c] = total
     total_copy, total_back = partner(pair.at[c], pair.at[1 - c], 2)
     total_copy.start()
-
     for d in range(1, fs):
         finish_dir(d)
     total_back.wait_recv()
@@ -996,21 +1007,16 @@
             new_out[:, columns] = new
             copies[x][own_block, columns] = new.astype(bf16)
 
-    def relay_last(k):
-        for n in range(3, fs):
-            relay_weight(k, other(n))
-
-    def finish_weight(n):
-        arrived(weight_query_all.at[pl.ds(0, quarter)], query_end_r.at[other(n)])
-
     finish_weight(1)
     copy_rows(0, other(1) * height, height)
     relay_last(0)
+    for d in range(2, fs - 1):
+        onward_all(key_z, d, 1)
+    for n in (1, 2):
+        copy_rows(1, other(n) * height, height)
+    relay_last(1)
     finish_weight(2)
     copy_rows(0, other(2) * height, height)
-    relay_last(1)
-    for n in (1, 2):
-        copy_rows(1, other(n) * height, height)
     for n in range(3, fs):
         for owner in (r, near, far):
             copy_rows(0, other(n) * height + owner * quarter, quarter)
@@ -1021,11 +1027,10 @@
     for n in range(3, fs):
         finish_weight(n)
         copy_rows(0, other(n) * height + across * quarter, quarter)
-    edge = (f == 0) | (f == fs - 1)
     hops = (fs - 1) * (rep - 1) * quarter
     for n, block in ((0, basis_all.at[c]), (1, weight_query_all)):
         departed(block.at[pl.ds(0, quarter)], line_s.at[n], edge)
-        departed(block.at[pl.ds(0, (fs + 1) * quarter)], line_s.at[n], jnp.logical_not(edge))
+        departed(block.at[pl.ds(0, (fs + 1) * quarter)], line_s.at[n], inner)
         departed(block.at[pl.ds(0, hops)], hop_s.at[n])
     for n in range(fs):
         if n < fs - 1:
@@ -1036,7 +1041,9 @@
     departed(pair_sum, halve_s.at[1])
     departed(slab_recv.at[pl.ds(0, fs - 1)], slab_s.at[0])
     departed(low_all.at[pl.ds(0, rep - 1)], low_s.at[0])
-    departed(slab_recv.at[pl.ds(0, fs - 1)], dir_s.at[0])
+    for x in range(2):
+        departed(directions[x].at[pl.ds(0, own)], dir_s.at[x], edge)
+        departed(directions[x].at[pl.ds(0, (fs + 1) * own)], dir_s.at[x], inner)
     for n in range(1, fs):
         departed(low_all.at[pl.ds(0, rep - 1)], dir_hop_s.at[n])
     departed(squares.at[pl.ds(0, fs - 1)], squares_s.at[0])
@@ -1046,11 +1053,14 @@
 
 def write_out(*refs):
     count = len(refs) // 2
-    copies = [
-        pltpu.make_async_copy(source, target, refs[-1].at[n])
-        for n, (source, target) in enumerate(zip(refs[:count], refs[count : 2 * count]))
-    ]
-    for copy in copies:
+    copies, starts = [], []
+    for n, (source, target) in enumerate(zip(refs[:count], refs[count : 2 * count])):
+        copies.append(pltpu.make_async_copy(source, target, refs[-1].at[n]))
+        size = source.shape[0] // 4 if source.ndim == 2 else 1
+        for start in range(0, source.shape[0], size):
+            span = pl.ds(start, size)
+            starts.append(pltpu.make_async_copy(source.at[span], target.at[span], refs[-1].at[n]))
+    for copy in starts:
         copy.start()
     for copy in copies:
         copy.wait()
@@ -1146,7 +1156,7 @@
         shape((2, rows, key_cols), f32),
     )
     own, units = rows // rep, (query_cols + key_cols) // LANES
-    if own % 16 == 0 and fs % 2 == 0 and fs > 2 and units % 2 == 0:
+    if own % 16 == 0 and fs == 4 and units % 2 == 0:
         fresh = pl.pallas_call(
             functools.partial(exchange_grid, fs, rep),
             out_shape=results,
@@ -1178,11 +1188,11 @@
                 pltpu.VMEM((2, 2, 8, LANES), f32),
                 dma((2,)),
                 dma((2,)),
-                dma((fs, 2)),
+                dma((fs, 4)),
                 dma((fs, 2)),
                 dma((fs,)),
                 dma((2,)),
-                dma((fs, 2)),
+                dma((fs, 4)),
                 dma((fs, 2)),
                 dma((1,)),
                 dma((fs,)),
@@ -1194,7 +1204,7 @@
                 dma((1,)),
                 dma((2,)),
                 dma((1,)),
-                dma((1,)),
+                dma((2,)),
                 dma((2, fs)),
                 dma((fs,)),
                 dma((fs, 2)),

time: 83.7 us -> 78.4 us (0.937)
  Pallas kernels: 82.9 us -> 77.6 us
    pallas_call x1, Pallas kernels: 78.5 us -> 73.2 us  [on_device(): pl.pallas_call(functools.partial(exchange_grid, fs, rep), out_shape=resul...]
where the time goes in v3:
time: 78.4 us; the launch traced here: 78.2 us
  Pallas kernels  77.6 us (99%)
    pallas_call x1, Pallas kernels, on_device(): pl.pallas_call(functools.partial(exchange_grid, fs, rep), out_shape=resul...  73.2 us
    pallas_call x1, Pallas kernels, on_device(): pl.pallas_call(write_out, out_shape=results, in_specs=[vmem] * 8, out_spe...  4.35 us

profile of v3, /device:TPU:0, one launch (start us, length us, event | category | flops | bytes accessed | tf_op | source)
XLA Modules:
  0.0 78.2 jit_solution(4885225521583504501)
XLA Ops:
  0.6 73.2 %shard_map.152 = (f32[512,1024]{1,0:T(8,128)S(1)}, f32[512,256]{1,0:T(8,128)S(1)}, f32[512,1024]{1,0:T(8,128)S(1)}, f32[512,256]{1,0:T(8,128)S(1)}, bf16[2048,10...) custom-call(bf16[256,2048]{1,0:T(8,128)(2,1)} %inputs_far.1, ...), custom_call_target="tpu_custom_call" | custom-call | tf_op jit(solution)/shard_map/pallas_call | solution.py:1160
  73.9 4.3 %shard_map.153 = (f32[512,1024]{1,0:T(8,128)}, f32[512,256]{1,0:T(8,128)}, f32[512,1024]{1,0:T(8,128)}, f32[512,256]{1,0:T(8,128)}, bf16[2048,1024]{1,0:T(8,128)...) custom-call(f32[512,1024]{1,0:T(8,128)S(1)} %get-tuple-element.16.refs_0_, ...), custom_call_target="tpu_custom_call" | custom-call | tf_op jit(solution)/shard_map/pallas_call | solution.py:1237

commit v4 on v3

--- a/solution.py
+++ b/solution.py
@@ -498,6 +498,8 @@
     part_squares,
     squares,
     pair,
+    late_query,
+    late_key,
     line_s,
     key_s,
     basis_line_r,
@@ -666,8 +668,9 @@
         return remote(block, block, line_s.at[1], query_line_r.at[source, k], fs=f + 2 * up - 1)
 
     def key_z(source, up, k):
-        block = weight_key_all.at[rows_of(source * height, height)]
-        return remote(block, block, key_s.at[up], key_line_r.at[source], fs=f + 2 * up - 1)
+        size = height // chunks
+        block = weight_key_all.at[rows_of(source * height + k * size, size)]
+        return remote(block, block, key_s.at[up], key_line_r.at[source, k], fs=f + 2 * up - 1)
 
     def launch(line, parts=chunks):
         for k in range(parts):
@@ -709,8 +712,9 @@
         for source, there in sources(d):
             relay_basis(k, source, there)
     onward_all(query_z, 1)
-    launch(key_z, 1)
+    launch(key_z)
     spread(functools.partial(weight_hop, 0), other(1))
+    spread(functools.partial(weight_hop, 1), other(1), c == 1)
     arrived(basis_all.at[c, pl.ds(0, (fs - 1) * quarter)], basis_end_r.at[0])
     for load in loads[2:]:
         load.wait()
@@ -813,8 +817,7 @@
     start_second(0)
     start_first(1, 1)
     start_second(1)
-    for k in range(1, chunks):
-        spread(functools.partial(weight_hop, k), other(1))
+    spread(functools.partial(weight_hop, 1), other(1), c == 0)
     end_rep(0)
     end_rep(1)
     for k in range(chunks):
@@ -946,7 +949,7 @@
     mine = squares.at[f]
     for n in range(1, fs):
         remote(mine, mine, squares_s.at[0], squares_r.at[0], fs=other(n)).start()
-    onward_all(key_z, 1, 1)
+    onward_all(key_z, 1)
     relay_dir(2)
     relay_dir(3)
     for n in range(3, fs):
@@ -973,6 +976,7 @@
         finish_dir(d)
     total_back.wait_recv()
     totals = pair[0] + pair[1]
+    onward(key_z, 2, 0)
     weights_all, copies = (weight_query_all, weight_key_all), (copy_query, copy_key)
     scales = [
         lax.rsqrt(jnp.sum(totals[x], keepdims=True) / (pair.shape[0] * rank * copies[x].shape[1]) + 1e-06)
@@ -988,6 +992,15 @@
         wide = copies[x].shape[1]
         width = 2 * LANES if wide % (2 * LANES) == 0 else LANES
         return [slice(n, n + width) for n in range(0, wide, width)]
+
+    def ahead_rows(x, start, size, held):
+        for columns in column_blocks(x):
+            held[pl.ds(0, size), columns] = 0.02 * product(x, rows_of(start, size), columns)
+
+    def late_rows(x, start, size, held):
+        span = rows_of(start, size)
+        weight = weights_all[x][span].astype(f32)
+        copies[x][span] = (weight - held[pl.ds(0, size)]).astype(bf16)
 
     def copy_rows(x, start, size):
         span = rows_of(start, size)
@@ -1010,23 +1023,25 @@
     finish_weight(1)
     copy_rows(0, other(1) * height, height)
     relay_last(0)
-    for d in range(2, fs - 1):
-        onward_all(key_z, d, 1)
+    onward(key_z, 2, 1)
     for n in (1, 2):
         copy_rows(1, other(n) * height, height)
     relay_last(1)
-    finish_weight(2)
-    copy_rows(0, other(2) * height, height)
     for n in range(3, fs):
         for owner in (r, near, far):
             copy_rows(0, other(n) * height + owner * quarter, quarter)
-    for d in range(max(fs - 1, 3), fs):
-        onward_all(key_z, d, 1)
     for n in range(3, fs):
-        copy_rows(1, other(n) * height, height)
+        ahead_rows(0, other(n) * height + across * quarter, quarter, late_query)
+        ahead_rows(1, other(n) * height, height, late_key)
+    finish_weight(2)
+    copy_rows(0, other(2) * height, height)
+    for d in range(3, fs):
+        onward_all(key_z, d)
+    for n in range(3, fs):
+        late_rows(1, other(n) * height, height, late_key)
     for n in range(3, fs):
         finish_weight(n)
-        copy_rows(0, other(n) * height + across * quarter, quarter)
+        late_rows(0, other(n) * height + across * quarter, quarter, late_query)
     hops = (fs - 1) * (rep - 1) * quarter
     for n, block in ((0, basis_all.at[c]), (1, weight_query_all)):
         departed(block.at[pl.ds(0, quarter)], line_s.at[n], edge)
@@ -1186,11 +1201,13 @@
                 pltpu.VMEM((rep, 2, 2, 8, LANES), f32),
                 pltpu.VMEM((fs, 2, 8, LANES), f32),
                 pltpu.VMEM((2, 2, 8, LANES), f32),
+                pltpu.VMEM((height // rep, query_cols), f32),
+                pltpu.VMEM((height, key_cols), f32),
                 dma((2,)),
                 dma((2,)),
                 dma((fs, 4)),
                 dma((fs, 2)),
-                dma((fs,)),
+                dma((fs, 2)),
                 dma((2,)),
                 dma((fs, 4)),
                 dma((fs, 2)),

time: 78.4 us -> 77.4 us (0.987)
  Pallas kernels: 77.6 us -> 76.6 us
    pallas_call x1, Pallas kernels: 73.2 us -> 72.2 us  [on_device(): pl.pallas_call(functools.partial(exchange_grid, fs, rep), out_shape=resul...]
where the time goes in v4:
time: 77.4 us; the launch traced here: 77.2 us
  Pallas kernels  76.6 us (99%)
    pallas_call x1, Pallas kernels, on_device(): pl.pallas_call(functools.partial(exchange_grid, fs, rep), out_shape=resul...  72.2 us
    pallas_call x1, Pallas kernels, on_device(): pl.pallas_call(write_out, out_shape=results, in_specs=[vmem] * 8, out_spe...  4.35 us

profile of v4, /device:TPU:0, one launch (start us, length us, event | category | flops | bytes accessed | tf_op | source)
XLA Modules:
  0.0 77.2 jit_solution(9943399963681299253)
XLA Ops:
  0.6 72.2 %shard_map.152 = (f32[512,1024]{1,0:T(8,128)S(1)}, f32[512,256]{1,0:T(8,128)S(1)}, f32[512,1024]{1,0:T(8,128)S(1)}, f32[512,256]{1,0:T(8,128)S(1)}, bf16[2048,10...) custom-call(bf16[256,2048]{1,0:T(8,128)(2,1)} %inputs_far.1, ...), custom_call_target="tpu_custom_call" | custom-call | tf_op jit(solution)/shard_map/pallas_call | solution.py:1175
  72.9 4.3 %shard_map.153 = (f32[512,1024]{1,0:T(8,128)}, f32[512,256]{1,0:T(8,128)}, f32[512,1024]{1,0:T(8,128)}, f32[512,256]{1,0:T(8,128)}, bf16[2048,1024]{1,0:T(8,128)...) custom-call(f32[512,1024]{1,0:T(8,128)S(1)} %get-tuple-element.16.refs_0_, ...), custom_call_target="tpu_custom_call" | custom-call | tf_op jit(solution)/shard_map/pallas_call | solution.py:1254

commit v5 on v4

--- a/solution.py
+++ b/solution.py
@@ -612,23 +612,28 @@
     for load in loads:
         load.start()
     own_basis = pltpu.make_async_copy(basis_query, basis_all.at[c, own_block], local.at[0])
+    ways = ((1, f + 1 < fs), (0, f > 0))
+    edge = (f == 0) | (f == fs - 1)
+    inner = (f > 0) & (f < fs - 1)
     barrier = pltpu.get_barrier_semaphore()
-    for i in range(1, fs):
+
+    def greet(up):
         pl.semaphore_signal(
-            barrier, inc=1, device_id={"fs": lax.rem(f + i, fs)}, device_id_type=MESH
-        )
+            barrier, inc=1, device_id={"fs": f + 2 * up - 1}, device_id_type=MESH
+        )
+
+    for up, there in ways:
+        when((there,), functools.partial(greet, up))
     for mate in (near, far):
         pl.semaphore_signal(barrier, inc=1, device_id={"rep": mate}, device_id_type=MESH)
     pl.semaphore_signal(barrier, inc=1, device_id={"tp": 1 - c}, device_id_type=MESH)
-    pl.semaphore_wait(barrier, fs + 2)
+    when((edge,), lambda: pl.semaphore_wait(barrier, 4))
+    when((inner,), lambda: pl.semaphore_wait(barrier, 5))
 
     def basis_z(source, up, k):
         block = basis_all.at[c, piece(source, r, k, fine)]
         return remote(block, block, line_s.at[0], basis_line_r.at[source, k], fs=f + 2 * up - 1)
 
-    ways = ((1, f + 1 < fs), (0, f > 0))
-    edge = (f == 0) | (f == fs - 1)
-    inner = (f > 0) & (f < fs - 1)
     def hop_span(slot, width):
         return (pl.ds(0, width), pl.ds(0, width), pl.ds(0, width // 2), pl.ds(width // 2, width // 2))[slot]
 
@@ -952,12 +957,12 @@
     onward_all(key_z, 1)
     relay_dir(2)
     relay_dir(3)
+    relay_weight(0, other(2))
     for n in range(3, fs):
         for k in range(chunks):
             onward(query_z, n, k)
             spread(functools.partial(weight_hop, k), other(n))
-    for k in range(chunks):
-        relay_weight(k, other(2))
+    relay_weight(1, other(2))
     def relay_last(k):
         for n in range(3, fs):
             relay_weight(k, other(n))

time: 77.4 us -> 76 us (0.982)
  Pallas kernels: 76.6 us -> 75.2 us
    pallas_call x1, Pallas kernels: 72.2 us -> 70.8 us  [on_device(): pl.pallas_call(functools.partial(exchange_grid, fs, rep), out_shape=resul...]
where the time goes in v5:
time: 76 us; the launch traced here: 75.8 us
  Pallas kernels  75.2 us (99%)
    pallas_call x1, Pallas kernels, on_device(): pl.pallas_call(functools.partial(exchange_grid, fs, rep), out_shape=resul...  70.8 us
    pallas_call x1, Pallas kernels, on_device(): pl.pallas_call(write_out, out_shape=results, in_specs=[vmem] * 8, out_spe...  4.35 us

profile of v5, /device:TPU:0, one launch (start us, length us, event | category | flops | bytes accessed | tf_op | source)
XLA Modules:
  0.0 75.8 jit_solution(13259058525323342578)
XLA Ops:
  0.6 70.8 %shard_map.152 = (f32[512,1024]{1,0:T(8,128)S(1)}, f32[512,256]{1,0:T(8,128)S(1)}, f32[512,1024]{1,0:T(8,128)S(1)}, f32[512,256]{1,0:T(8,128)S(1)}, bf16[2048,10...) custom-call(bf16[256,2048]{1,0:T(8,128)(2,1)} %inputs_far.1, ...), custom_call_target="tpu_custom_call" | custom-call | tf_op jit(solution)/shard_map/pallas_call | solution.py:1180
  71.4 4.3 %shard_map.153 = (f32[512,1024]{1,0:T(8,128)}, f32[512,256]{1,0:T(8,128)}, f32[512,1024]{1,0:T(8,128)}, f32[512,256]{1,0:T(8,128)}, bf16[2048,1024]{1,0:T(8,128)...) custom-call(f32[512,1024]{1,0:T(8,128)S(1)} %get-tuple-element.16.refs_0_, ...), custom_call_target="tpu_custom_call" | custom-call | tf_op jit(solution)/shard_map/pallas_call | solution.py:1259

commit v6 on v5

--- a/solution.py
+++ b/solution.py
@@ -882,9 +882,9 @@
             remote(block, block, dir_s.at[x], dir_r.at[g, source], fs=f + 2 * up - 1).start()
 
     def dir_hop(g, slot, n):
-        landed = dir_hop_r.at[n, g] if slot == g else dir_end_r.at[n]
+        landed = dir_hop_r.at[n - 1, g] if slot == g else dir_end_r.at[0]
         for x, block in dir_blocks(g, other(n), sent[slot]):
-            remote(block, block, dir_hop_s.at[n], landed, rep=targets[slot]).start()
+            remote(block, block, dir_hop_s.at[0], landed, rep=targets[slot]).start()
 
     def end_fs(g):
         arrived(slab_recv.at[pl.ds(0, fs - 1), columns_of(g)], slab_r.at[g])
@@ -919,11 +919,8 @@
 
     def relay_dir(n):
         for g in range(2):
-            arrived(low_all.at[r, columns_of(g)], dir_hop_r.at[n, g])
+            arrived(low_all.at[r, columns_of(g)], dir_hop_r.at[n - 1, g])
             dir_hop(g, g + 2, n)
-
-    def finish_dir(n):
-        arrived(low_all.at[pl.ds(0, 2)], dir_end_r.at[n])
 
     for k in range(chunks):
         relay_weight(k, other(1))
@@ -977,8 +974,7 @@
     pair[c] = total
     total_copy, total_back = partner(pair.at[c], pair.at[1 - c], 2)
     total_copy.start()
-    for d in range(1, fs):
-        finish_dir(d)
+    arrived(part.at[:, pl.ds(0, fs - 1), pl.ds(0, 2 * own)], dir_end_r.at[0])
     total_back.wait_recv()
     totals = pair[0] + pair[1]
     onward(key_z, 2, 0)
@@ -1064,8 +1060,7 @@
     for x in range(2):
         departed(directions[x].at[pl.ds(0, own)], dir_s.at[x], edge)
         departed(directions[x].at[pl.ds(0, (fs + 1) * own)], dir_s.at[x], inner)
-    for n in range(1, fs):
-        departed(low_all.at[pl.ds(0, rep - 1)], dir_hop_s.at[n])
+    departed(part.at[:, pl.ds(0, fs - 1), pl.ds(0, (rep - 1) * own)], dir_hop_s.at[0])
     departed(squares.at[pl.ds(0, fs - 1)], squares_s.at[0])
     for copy in (factor_copy, swap, total_copy):
         copy.wait_send()
@@ -1228,9 +1223,9 @@
                 dma((1,)),
                 dma((2,)),
                 dma((2, fs)),
-                dma((fs,)),
-                dma((fs, 2)),
-                dma((fs,)),
+                dma((1,)),
+                dma((fs - 1, 2)),
+                dma((1,)),
                 dma((1,)),
                 dma((1,)),
                 dma((3,)),

time: 76 us -> 75.9 us (level)
  no operation moved by 1% of the time
where the time goes in v6:
time: 75.9 us; the launch traced here: 75.7 us
  Pallas kernels  75.1 us (99%)
    pallas_call x1, Pallas kernels, on_device(): pl.pallas_call(functools.partial(exchange_grid, fs, rep), out_shape=resul...  70.7 us
    pallas_call x1, Pallas kernels, on_device(): pl.pallas_call(write_out, out_shape=results, in_specs=[vmem] * 8, out_spe...  4.35 us

profile of v6, /device:TPU:0, one launch (start us, length us, event | category | flops | bytes accessed | tf_op | source)
XLA Modules:
  0.0 75.7 jit_solution(15608459611868023358)
XLA Ops:
  0.6 70.7 %shard_map.152 = (f32[512,1024]{1,0:T(8,128)S(1)}, f32[512,256]{1,0:T(8,128)S(1)}, f32[512,1024]{1,0:T(8,128)S(1)}, f32[512,256]{1,0:T(8,128)S(1)}, bf16[2048,10...) custom-call(bf16[256,2048]{1,0:T(8,128)(2,1)} %inputs_far.1, ...), custom_call_target="tpu_custom_call" | custom-call | tf_op jit(solution)/shard_map/pallas_call | solution.py:1175
  71.4 4.3 %shard_map.153 = (f32[512,1024]{1,0:T(8,128)}, f32[512,256]{1,0:T(8,128)}, f32[512,1024]{1,0:T(8,128)}, f32[512,256]{1,0:T(8,128)}, bf16[2048,1024]{1,0:T(8,128)...) custom-call(f32[512,1024]{1,0:T(8,128)S(1)} %get-tuple-element.16.refs_0_, ...), custom_call_target="tpu_custom_call" | custom-call | tf_op jit(solution)/shard_map/pallas_call | solution.py:1254
